TPU v7x, 128 devices: a whole 4x4x4 slice. The times are simulated.
128 devices in a mesh: sp: 16 (over z, x), tp: 8 (over y, core).
Axes of the slice: x: 4, y: 4, z: 4, core: 2. Of those that a mesh axis runs over, the one named last changes fastest.
Arguments:
- queries: bfloat16 [16384, 512], P('sp', 'tp'), may hold values from -16 to 16
- key_heads: bfloat16 [16384, 512], P('sp', 'tp'), may hold values from -16 to 16
- value_heads: bfloat16 [16384, 512], P('sp', 'tp'), may hold values from -6 to 6
- head_gain: float32 [512], P('tp'), may hold values from 0.1 to 1.9
- residual: bfloat16 [16384, 2048], P(('sp', 'tp')), may hold values from -6 to 6
- out_weight: bfloat16 [512, 2048], replicated, may hold values from -0.25 to 0.25
- norm_gain: float32 [2048], replicated, may hold values from 0.1 to 1.9
- shared_gate: bfloat16 [2048, 512], replicated, may hold values from -0.125 to 0.125
- shared_up: bfloat16 [2048, 512], replicated, may hold values from -0.125 to 0.125
- shared_down: bfloat16 [512, 2048], replicated, may hold values from -0.25 to 0.25
- expert_gate: bfloat16 [256, 2048, 512], P(('sp', 'tp')), may hold values from -0.125 to 0.125
- expert_up: bfloat16 [256, 2048, 512], P(('sp', 'tp')), may hold values from -0.125 to 0.125
- expert_down: bfloat16 [256, 512, 2048], P(('sp', 'tp')), may hold values from -0.25 to 0.25
- routed_experts: int32 [16384, 4], P(('sp', 'tp')), may hold values from 0 to 255, all different within a row; in each aligned block of 128 rows (0 to 127, 128 to 255, ...) at most 3 rows name the same one
- route_weights: float32 [16384, 4], P(('sp', 'tp')), may hold values from 0.1 to 1.5
Outputs:
- layer_output: bfloat16 [16384, 2048], P(('sp', 'tp'))
Inputs may be any that keep to these rules, and one draw needn't show every extreme that they name: `routed_experts`: each row names 4 different experts. Within the rows of one device (128 consecutive rows, aligned) no expert is named more than 3 times, and in every draw some expert is named exactly 3 times in some device's rows.
All inputs are finite; a program needn't handle non-finite values.
Results may differ from a plain program's by a relative error of at most 0.014.
Values may be sent and summed in bfloat16 or wider, within the bound.
A program may use at most 128 MiB of HBM per device.

v0:
```python
import math

import jax
import jax.numpy as jnp
from jax import lax
from jax.sharding import PartitionSpec as P

HEAD_DIM = 64


EPSILON = 1e-06


def side_by_side(arrays, axis, dim, along):
    widths = [a.shape[along] for a in arrays]
    both = jnp.concatenate(arrays, axis=along)
    whole = lax.all_gather(both, axis, axis=dim, tiled=True)
    return tuple(jnp.split(whole, [sum(widths[:k]) for k in range(1, len(widths))], axis=along))


def block_terms(query_block, key_block, value_block, query_start, key_start):
    scale = 1.0 / math.sqrt(HEAD_DIM)
    scores = (
        jnp.einsum("qhd,khd->hqk", query_block, key_block, preferred_element_type=jnp.float32)
        * scale
    )
    query_places = query_start + lax.iota(jnp.int32, query_block.shape[0])
    key_places = key_start + lax.iota(jnp.int32, key_block.shape[0])
    earlier = (key_places[None, :] < query_places[:, None])[None]
    stay_log = jnp.where(earlier, jax.nn.log_sigmoid(-scores), 0.0)
    after_log = lax.cumsum(stay_log, axis=2, reverse=True) - stay_log
    weights = jnp.where(earlier, jnp.exp(jax.nn.log_sigmoid(scores) + after_log), 0.0).astype(
        jnp.bfloat16
    )
    partial_out = jnp.einsum(
        "hqk,khd->qhd", weights, value_block, preferred_element_type=jnp.float32
    )
    block_total = jnp.transpose(jnp.sum(stay_log, axis=2))
    return (block_total, partial_out)


def head_norm(mixed, head_gain):
    inverse = lax.rsqrt(jnp.mean(mixed * mixed, axis=2, keepdims=True) + EPSILON)
    normed = mixed * inverse * head_gain.reshape(mixed.shape[1], mixed.shape[2])
    return normed.reshape(mixed.shape[0], -1).astype(jnp.bfloat16)


def stick_breaking(queries, key_heads, value_heads):
    seq_count = queries.shape[0]
    head_count = queries.shape[1] // HEAD_DIM
    shard_count = lax.axis_size("sp")
    shard_place = lax.axis_index("sp")
    query_width = 512
    query_blocks = queries.reshape(seq_count // query_width, query_width, head_count, HEAD_DIM)
    block_starts = shard_place * seq_count + query_width * jnp.arange(
        seq_count // query_width, dtype=jnp.int32
    )

    def shard_terms(key_block, value_block, key_start):

        def one_block(inputs):
            query_block, query_start = inputs
            return block_terms(query_block, key_block, value_block, query_start, key_start)

        totals, partials = lax.map(one_block, (query_blocks, block_starts))
        return (
            totals.reshape(seq_count, head_count),
            partials.reshape(seq_count, head_count, HEAD_DIM),
        )

    initial = (
        jnp.zeros((shard_count, seq_count, head_count), jnp.float32),
        jnp.zeros((shard_count, seq_count, head_count, HEAD_DIM), jnp.float32),
    )
    pieces = side_by_side((key_heads, value_heads), "sp", 0, 1)
    key_piece = pieces[0].reshape(-1, seq_count, head_count, HEAD_DIM)
    value_piece = pieces[1].reshape(-1, seq_count, head_count, HEAD_DIM)

    def add_one(shard_step, state):
        total_store, partial_store = state
        key_block = lax.dynamic_index_in_dim(key_piece, shard_step, 0, keepdims=False)
        value_block = lax.dynamic_index_in_dim(value_piece, shard_step, 0, keepdims=False)

        def compute(unused):
            return shard_terms(key_block, value_block, shard_step * seq_count)

        def nothing(unused):
            return (
                jnp.zeros((seq_count, head_count), jnp.float32),
                jnp.zeros((seq_count, head_count, HEAD_DIM), jnp.float32),
            )

        totals, partials = lax.cond(shard_step <= shard_place, compute, nothing, 0)
        total_store = lax.dynamic_update_index_in_dim(total_store, totals, shard_step, 0)
        partial_store = lax.dynamic_update_index_in_dim(partial_store, partials, shard_step, 0)
        return (total_store, partial_store)

    totals, partials = lax.fori_loop(0, key_piece.shape[0], add_one, initial)
    later = lax.cumsum(totals, axis=0, reverse=True) - totals
    return jnp.sum(jnp.exp(later)[..., None] * partials, axis=0)


def routed_sum(expert_input, expert_gate, expert_up, expert_down, routed_experts, route_weights):
    row_count, pick_count = routed_experts.shape
    local_experts = expert_gate.shape[0]
    model_width = expert_input.shape[1]
    sp_count = lax.axis_size("sp")
    tp_count = lax.axis_size("tp")
    device_count = sp_count * tp_count
    expert_count = local_experts * device_count
    capacity = max(2, 3 * row_count * pick_count // (2 * expert_count))
    flat_experts = routed_experts.reshape(-1)
    expert_table = (
        flat_experts[:, None] == jnp.arange(expert_count, dtype=jnp.int32)[None, :]
    ).astype(jnp.int32)
    ranking = jnp.sum(jnp.cumsum(expert_table, axis=0) * expert_table, axis=1) - 1
    holder = flat_experts // local_experts
    resident = flat_experts % local_experts
    slot_index = (resident * device_count + holder) * capacity + ranking
    placement = (
        slot_index[:, None] == jnp.arange(expert_count * capacity, dtype=jnp.int32)[None, :]
    ).astype(jnp.bfloat16)
    token_place = jnp.sum(placement.reshape(row_count, pick_count, -1), axis=1)
    outgoing = jnp.einsum(
        "rs,rd->sd", token_place, expert_input, preferred_element_type=jnp.float32
    ).astype(jnp.bfloat16)
    outgoing = outgoing.reshape(local_experts, device_count, capacity, model_width)
    arrived = lax.all_to_all(outgoing, ("sp", "tp"), split_axis=1, concat_axis=1, tiled=True)
    grouped = arrived.reshape(local_experts, -1, model_width)
    gate_part = jnp.einsum("erd,edf->erf", grouped, expert_gate, preferred_element_type=jnp.float32)
    up_part = jnp.einsum("erd,edf->erf", grouped, expert_up, preferred_element_type=jnp.float32)
    hidden = (jax.nn.silu(gate_part) * up_part).astype(jnp.bfloat16)
    result = jnp.einsum(
        "erf,efd->erd", hidden, expert_down, preferred_element_type=jnp.float32
    ).astype(jnp.bfloat16)
    returned = lax.all_to_all(
        result.reshape(arrived.shape), ("sp", "tp"), split_axis=1, concat_axis=1, tiled=True
    )
    gathered = jnp.dot(
        placement, returned.reshape(-1, model_width), preferred_element_type=jnp.float32
    )
    weighted = gathered.reshape(row_count, pick_count, model_width) * route_weights[:, :, None]
    return jnp.sum(weighted, axis=1)


def body(
    queries,
    key_heads,
    value_heads,
    head_gain,
    residual,
    out_weight,
    norm_gain,
    shared_gate,
    shared_up,
    shared_down,
    expert_gate,
    expert_up,
    expert_down,
    routed_experts,
    route_weights,
):
    head_output = head_norm(stick_breaking(queries, key_heads, value_heads), head_gain)
    token_heads = lax.all_to_all(head_output, "tp", split_axis=0, concat_axis=1, tiled=True)
    branch = jnp.dot(token_heads, out_weight, preferred_element_type=jnp.float32)
    stream = (residual.astype(jnp.float32) + branch).astype(jnp.bfloat16)
    stream_wide = stream.astype(jnp.float32)
    inverse = lax.rsqrt(jnp.mean(stream_wide * stream_wide, axis=1, keepdims=True) + EPSILON)
    expert_input = (stream_wide * inverse * norm_gain).astype(jnp.bfloat16)
    shared_hidden = (
        jax.nn.silu(jnp.dot(expert_input, shared_gate, preferred_element_type=jnp.float32))
        * jnp.dot(expert_input, shared_up, preferred_element_type=jnp.float32)
    ).astype(jnp.bfloat16)
    shared_term = jnp.dot(shared_hidden, shared_down, preferred_element_type=jnp.float32)
    routed = routed_sum(
        expert_input, expert_gate, expert_up, expert_down, routed_experts, route_weights
    )
    return (stream_wide + shared_term + routed).astype(jnp.bfloat16)


def solution(mesh):
    return jax.shard_map(
        body,
        mesh=mesh,
        in_specs=(
            P("sp", "tp"),
            P("sp", "tp"),
            P("sp", "tp"),
            P("tp"),
            P(("sp", "tp"), None),
            P(),
            P(),
            P(),
            P(),
            P(),
            P(("sp", "tp"), None, None),
            P(("sp", "tp"), None, None),
            P(("sp", "tp"), None, None),
            P(("sp", "tp"), None),
            P(("sp", "tp"), None),
        ),
        out_specs=P(("sp", "tp"), None),
        check_vma=False,
    )
```

profile of v0, /device:TPU:1, one launch (start us, length us, event | category | flops | bytes accessed | tf_op | source)
XLA Modules:
  0.0 1197.8 jit_solution(7784886853895001931)
XLA Ops:
  6.5 1.8 pad_maximum_fusion
  9.5 1.0 reshape.268
  12.1 52.0 %all-gather.2.cloned.1.call-done = bf16[16384,128]{0,1:T(8,128)(2,1)} async-done(((bf16[1024,128]{0,1:T(8,128)(2,1)}), bf16[16384,128]{0,1:T(8,128)(2,1)}) %all-gather.2.cloned.1.call-update) | async-done | bytes 4194320 | tf_op jit(solution)/shard_map/all_gather | solution.py:17
  64.0 2.6 fusion.59
  66.6 1.2 copy.148
  67.8 2.5 copy.127
  70.4 1.2 copy.149
  71.6 2.4 copy.128
  74.1 93.8 %while.37 = (s32[]{:T(128)}, f32[16,1024,1]{1,2,0:T(1,128)S(1)}, f32[16,1024,1,64]{3,2,1,0:T(1,128)}, s32[]{:T(128)}, bf16[16,1024,1,64]{1,3,2,0:T(8,128)(2,1)},...) while((s32[]{:T(128)}, f32[16,1024,1]{1,2,0:T(1,128)S(1)}, ...), condition=%wide.region_8.9_spmd.clone, body=%wide.region_0.8_spmd.clone.sunk | while | flops 218661376 | bytes 50712044 | solution.py:98
  74.2 56.0 %conditional.3 = (f32[1,1024,1]{1,2,0:T(1,128)}, f32[1,1024,1,64]{3,2,1,0:T(1,128)S(1)}) conditional(s32[]{:T(128)} %convert_element_type.95, () %tuple.76, (bf16[16,1024,1,64]{1,3,2,0:T(8,128)(2,1)}, s32[]{:T(128)}, bf16[16,1024,1,64]{1,3,2,0:T(8,128)(2,1)}, s32[]{:T(128)}, bf16[2,512,1,64]{1,3,2,0:T(8,128)(2,1)S(1)}, ...), branch_computations={%region_1.1_spmd, %region_2.7_spmd.clone} | conditional | flops 218661376 | bytes 49916744 | solution.py:93
  74.2 1.0 dynamic-slice_bitcast_fusion
  75.3 54.8 %while.36 = (s32[]{:T(128)}, f32[2,512,1]{1,2,0:T(1,128)}, f32[2,512,1,64]{1,3,2,0:T(8,128)S(1)}, s32[]{:T(128)}, s32[2]{0:T(128)S(1)}, /*index=5*/bf16[2,512,1,...) while((s32[]{:T(128)}, f32[2,512,1]{1,2,0:T(1,128)}, ...), condition=%wide.region_7.6_spmd, body=%wide.region_3.5_spmd.sunk | while | flops 218661376 | bytes 48868028 | solution.py:65
  77.2 1.5 fusion.88
  78.7 1.8 copy.172
  80.5 3.2 copy.173
  83.7 5.9 fusion.89
  89.6 1.3 copy-done.1
  91.1 1.9 broadcast.232
  93.0 3.1 copy.175
  96.2 5.9 fusion.90
  104.5 1.5 fusion.88
  106.1 1.8 copy.172
  107.9 3.2 copy.173
  111.1 5.9 fusion.89
  117.0 1.3 copy-done.1
  118.5 1.9 broadcast.232
  120.4 3.1 copy.175
  123.6 5.9 fusion.90
  131.8 0.9 conditional.3
  168.1 21.6 %multiply_reduce_fusion = f32[1024,64]{1,0:T(8,128)S(1)} fusion(f32[16,1024,1,64]{3,2,1,0:T(1,128)} %get-tuple-element.244, f32[16,1024]{1,0:T(8,128)S(1)} %bitcast.147), kind=kLoop, calls=%fused_computation.34 | loop fusion | flops 2031616 | bytes 4521984 | tf_op jit(solution)/shard_map/reduce_sum | solution.py:100
  191.0 5.3 all-to-all-start
  196.5 5.0 all-to-all-done
  201.5 1.6 multiply_reduce_fusion.2
  203.1 2.7 convolution_convert_fusion.1
  205.9 9.1 reshape.270
  215.0 8.5 copy.137
  223.5 874.3 %all_to_all.26 = bf16[2,128,3,2048]{3,0,2,1:T(2,128)(2,1)S(1)} all-to-all(bf16[2,128,3,2048]{3,0,2,1:T(2,128)(2,1)S(1)} %copy.137), channel_id=1, replica_groups=mesh['sp'=16,'tp'=8] {'sp','tp'}, dimensions={1} | all-to-all | bytes 6291456 | tf_op jit(solution)/shard_map/all_to_all | solution.py:128
  1097.7 1.7 copy-done.3
  1099.4 3.2 fusion.22
  1102.7 10.3 convolution_convert_fusion
  1113.0 6.8 copy.140
  1119.8 5.7 all-to-all-start.2
  1125.6 2.1 fusion.58
  1127.7 39.3 %all-to-all-done.2 = bf16[2,128,3,2048]{3,0,2,1:T(2,128)(2,1)} async-done(((bf16[2,128,3,2048]{3,0,2,1:T(2,128)(2,1)}), bf16[2,128,3,2048]{3,0,2,1:T(2,128)(2,1)}, u32[]{:S(2)}, u32[]{:S(2)}) %all-to-all-start.2) | async-done | bytes 3145760 | tf_op jit(solution)/shard_map/all_to_all | solution.py:136
  1166.9 6.0 copy.141
  1173.0 8.8 reshape.274
  1181.8 4.8 multiply_reduce_fusion.1
  1186.6 4.2 fusion.27
  (165 shorter events, 59.5 us)
Async XLA Ops:
  6.5 195.0 %copy-start = (bf16[512,2048]{1,0:T(8,128)(2,1)S(1)}, bf16[512,2048]{1,0:T(8,128)(2,1)}, u32[]{:S(2)}) copy-start(bf16[512,2048]{1,0:T(8,128)(2,1)} %param.26) | copy-start | bytes 6291460
  6.5 57.5 %all-gather.2.cloned.1.call-start = ((), (), s32[]{:S(2)}) async-start(), calls=%async_computation.3 | async-start | bytes 4456448 | tf_op jit(solution)/shard_map/all_gather | solution.py:17
  8.4 3.1 copy-start.6
  75.7 2.9 copy-start.2
  89.6 1.3 copy-start.1
  103.1 2.9 copy-start.2
  117.0 1.3 copy-start.1
  168.1 22.1 %copy-start.7 = (f32[64]{0:T(128)S(1)}, f32[64]{0:T(128)}, u32[]{:S(2)}) copy-start(f32[64]{0:T(128)} %param.24) | copy-start | bytes 772
  189.8 6.5 copy-start.5
  191.0 12.1 %copy-start.4 = (f32[2048]{0:T(1024)S(1)}, f32[2048]{0:T(1024)}, u32[]{:S(2)}) copy-start(f32[2048]{0:T(1024)} %param.27) | copy-start | bytes 24580
  191.0 10.5 all-to-all-start
  223.4 876.0 %copy-start.8 = (bf16[2,2048,512]{2,1,0:T(8,128)(2,1)S(1)}, bf16[2,2048,512]{2,1,0:T(8,128)(2,1)}, u32[]{:S(2)}) copy-start(bf16[2,2048,512]{2,1,0:T(8,128)(2,1)} %param.31) | copy-start | bytes 12582916
  1097.7 1.7 copy-start.3
  1119.8 47.1 %all-to-all-start.2 = ((bf16[2,128,3,2048]{3,0,2,1:T(2,128)(2,1)}), bf16[2,128,3,2048]{3,0,2,1:T(2,128)(2,1)}, u32[]{:S(2)}, u32[]{:S(2)}) async-start(bf16[2,128,3,2048]{3,0,2,1:T(2,128)(2,1)} %bitcast.135), calls=%async_computation.2 | async-start | bytes 6291456 | tf_op jit(solution)/shard_map/all_to_all | solution.py:136
  1173.0 8.8 copy-start.9
Sparse Core Ops, SparseCore 0:
  9.5 54.5 all-gather.1
where the time goes:
time: 1210 us; the launch traced here: 1200 us
  blocking collectives  874 us (72%)
  local copies, waits for them, and re-layouts  119 us (10%)
  waiting for transfers between devices  96.3 us (8%)
  other arithmetic  41.6 us (3%)
  matrix products  41.6 us (3%)
  between operations  13.8 us (1%)
    all_to_all x1, blocking collectives, routed_sum(): lax.all_to_all(outgoing, ('sp', 'tp'), split_axis=1, concat_axis=1, tiled...  874 us
    all_gather x1, waiting for transfers between devices, side_by_side(): whole = lax.all_gather(both, axis, axis=dim, tiled=True)  52 us
    all_to_all x1, waiting for transfers between devices, routed_sum(): lax.all_to_all(result.reshape(arrived.shape), ('sp', 'tp'), split_axis=1,...  39.3 us
  transfers between devices with their start and end apart: 3, of which 3 were waited for; matrix products, arithmetic and copies ran while one was open for 0% of the time, Pallas kernels for 0%

commit v1 on v0

v1 whole, which is shorter than its diff:
```python
import math

import jax
import jax.numpy as jnp
from jax import lax
from jax.experimental import pallas as pl
from jax.experimental.pallas import tpu as pltpu
from jax.sharding import PartitionSpec as P

HEAD_DIM = 64


EPSILON = 1e-06


LOG2E = 1.4426950408889634
TILE = 256


def tile_terms(q2, keys, values, tri, carry, mask):
    x = jnp.dot(q2, keys, preferred_element_type=jnp.float32)
    drop = jnp.maximum(jnp.log(1.0 + jnp.exp2(jnp.minimum(x, 126.0))) * LOG2E, x)
    stick = x - drop
    if mask is not None:
        drop = jnp.where(mask, drop, 0.0)
    after = jnp.dot(drop.astype(jnp.bfloat16), tri, preferred_element_type=jnp.float32)
    both = jnp.concatenate([carry, carry], axis=1)
    weights = jnp.exp2(stick - after - both)
    if mask is not None:
        weights = jnp.where(mask, weights, 0.0)
    out = jnp.dot(weights.astype(jnp.bfloat16), values, preferred_element_type=jnp.float32)
    total = after[:, :1] + drop[:, :1]
    return out, carry + jnp.broadcast_to(total, carry.shape)


def attention_kernel(q_ref, kv_ref, gain_ref, out_ref, q2_ref, acc_ref, carry_ref, tri_ref):
    me = lax.axis_index("sp")
    q = q_ref[...].astype(jnp.float32) * (LOG2E / math.sqrt(HEAD_DIM))
    high = q.astype(jnp.bfloat16)
    low = (q - high.astype(jnp.float32)).astype(jnp.bfloat16)
    q2_ref[...] = jnp.concatenate([high, low], axis=1)
    row = lax.broadcasted_iota(jnp.int32, (TILE, TILE), 0)
    column = lax.broadcasted_iota(jnp.int32, (TILE, TILE), 1)
    tri_ref[...] = (row > column).astype(jnp.float32).astype(jnp.bfloat16)
    acc_ref[...] = jnp.zeros_like(acc_ref)
    carry_ref[...] = jnp.zeros_like(carry_ref)
    tiles = q_ref.shape[0] // TILE

    def chunk(block, part):
        left = kv_ref[block, pl.ds(part * 128, 64), :]
        right = kv_ref[block, pl.ds(part * 128 + 64, 64), :]
        keys = jnp.concatenate([left, right], axis=1)
        keys = jnp.concatenate([keys, keys], axis=0)
        values = kv_ref[block, pl.ds(512 + (part % 2) * TILE, TILE), :]
        side = lax.broadcasted_iota(jnp.int32, values.shape, 1) // HEAD_DIM
        return keys, jnp.where(side == part // 2, values, jnp.zeros_like(values))

    def add(tile, keys, values, mask):
        rows = pl.ds(tile * TILE, TILE)
        out, carry = tile_terms(
            q2_ref[rows, :], keys, values, tri_ref[...], carry_ref[rows, :], mask
        )
        acc_ref[rows, :] += out
        carry_ref[rows, :] = carry

    for part in range(tiles - 1, -1, -1):
        keys, values = chunk(me, part)
        for tile in range(part, tiles):
            add(tile, keys, values, column < row if tile == part else None)

    def step(i, unused):
        keys, values = chunk(me - 1 - i // tiles, tiles - 1 - i % tiles)
        for tile in range(tiles):
            add(tile, keys, values, None)
        return unused

    lax.fori_loop(0, me * tiles, step, 0)
    mixed = acc_ref[:, :HEAD_DIM] + acc_ref[:, HEAD_DIM:]
    inverse = lax.rsqrt(jnp.mean(mixed * mixed, axis=1, keepdims=True) + EPSILON)
    out_ref[...] = (mixed * inverse * gain_ref[...]).astype(jnp.bfloat16)


def pack_keys_values(key_heads, value_heads):
    rows = key_heads.shape[0]
    keys = key_heads.reshape(rows // 128, 128, HEAD_DIM).transpose(0, 2, 1).reshape(-1, 128)
    values = value_heads.reshape(2, rows // 2, HEAD_DIM).transpose(1, 0, 2).reshape(-1, 128)
    return jnp.concatenate([keys, values], axis=0)


def attention(queries, key_heads, value_heads, head_gain):
    rows = queries.shape[0]
    packed = pack_keys_values(key_heads, value_heads)
    everyone = lax.all_gather(packed, "sp", axis=0, tiled=False)
    return pl.pallas_call(
        attention_kernel,
        out_shape=jax.ShapeDtypeStruct((rows, HEAD_DIM), jnp.bfloat16),
        in_specs=[pl.BlockSpec(memory_space=pltpu.VMEM)] * 3,
        out_specs=pl.BlockSpec(memory_space=pltpu.VMEM),
        scratch_shapes=[
            pltpu.VMEM((rows, 128), jnp.bfloat16),
            pltpu.VMEM((rows, 128), jnp.float32),
            pltpu.VMEM((rows, 128), jnp.float32),
            pltpu.VMEM((TILE, TILE), jnp.bfloat16),
        ],
        compiler_params=pltpu.CompilerParams(vmem_limit_bytes=40 << 20),
        name="attention",
    )(queries, everyone, head_gain.reshape(1, HEAD_DIM))


def routed_sum(expert_input, expert_gate, expert_up, expert_down, routed_experts, route_weights):
    row_count, pick_count = routed_experts.shape
    local_experts = expert_gate.shape[0]
    model_width = expert_input.shape[1]
    sp_count = lax.axis_size("sp")
    tp_count = lax.axis_size("tp")
    device_count = sp_count * tp_count
    expert_count = local_experts * device_count
    capacity = max(2, 3 * row_count * pick_count // (2 * expert_count))
    flat_experts = routed_experts.reshape(-1)
    expert_table = (
        flat_experts[:, None] == jnp.arange(expert_count, dtype=jnp.int32)[None, :]
    ).astype(jnp.int32)
    ranking = jnp.sum(jnp.cumsum(expert_table, axis=0) * expert_table, axis=1) - 1
    holder = flat_experts // local_experts
    resident = flat_experts % local_experts
    slot_index = (resident * device_count + holder) * capacity + ranking
    placement = (
        slot_index[:, None] == jnp.arange(expert_count * capacity, dtype=jnp.int32)[None, :]
    ).astype(jnp.bfloat16)
    token_place = jnp.sum(placement.reshape(row_count, pick_count, -1), axis=1)
    outgoing = jnp.einsum(
        "rs,rd->sd", token_place, expert_input, preferred_element_type=jnp.float32
    ).astype(jnp.bfloat16)
    outgoing = outgoing.reshape(local_experts, device_count, capacity, model_width)
    arrived = lax.all_to_all(outgoing, ("sp", "tp"), split_axis=1, concat_axis=1, tiled=True)
    grouped = arrived.reshape(local_experts, -1, model_width)
    gate_part = jnp.einsum("erd,edf->erf", grouped, expert_gate, preferred_element_type=jnp.float32)
    up_part = jnp.einsum("erd,edf->erf", grouped, expert_up, preferred_element_type=jnp.float32)
    hidden = (jax.nn.silu(gate_part) * up_part).astype(jnp.bfloat16)
    result = jnp.einsum(
        "erf,efd->erd", hidden, expert_down, preferred_element_type=jnp.float32
    ).astype(jnp.bfloat16)
    returned = lax.all_to_all(
        result.reshape(arrived.shape), ("sp", "tp"), split_axis=1, concat_axis=1, tiled=True
    )
    gathered = jnp.dot(
        placement, returned.reshape(-1, model_width), preferred_element_type=jnp.float32
    )
    weighted = gathered.reshape(row_count, pick_count, model_width) * route_weights[:, :, None]
    return jnp.sum(weighted, axis=1)


def body(
    queries,
    key_heads,
    value_heads,
    head_gain,
    residual,
    out_weight,
    norm_gain,
    shared_gate,
    shared_up,
    shared_down,
    expert_gate,
    expert_up,
    expert_down,
    routed_experts,
    route_weights,
):
    head_output = attention(queries, key_heads, value_heads, head_gain)
    token_heads = lax.all_to_all(head_output, "tp", split_axis=0, concat_axis=1, tiled=True)
    branch = jnp.dot(token_heads, out_weight, preferred_element_type=jnp.float32)
    stream = (residual.astype(jnp.float32) + branch).astype(jnp.bfloat16)
    stream_wide = stream.astype(jnp.float32)
    inverse = lax.rsqrt(jnp.mean(stream_wide * stream_wide, axis=1, keepdims=True) + EPSILON)
    expert_input = (stream_wide * inverse * norm_gain).astype(jnp.bfloat16)
    shared_hidden = (
        jax.nn.silu(jnp.dot(expert_input, shared_gate, preferred_element_type=jnp.float32))
        * jnp.dot(expert_input, shared_up, preferred_element_type=jnp.float32)
    ).astype(jnp.bfloat16)
    shared_term = jnp.dot(shared_hidden, shared_down, preferred_element_type=jnp.float32)
    routed = routed_sum(
        expert_input, expert_gate, expert_up, expert_down, routed_experts, route_weights
    )
    return (stream_wide + shared_term + routed).astype(jnp.bfloat16)


def solution(mesh):
    return jax.shard_map(
        body,
        mesh=mesh,
        in_specs=(
            P("sp", "tp"),
            P("sp", "tp"),
            P("sp", "tp"),
            P("tp"),
            P(("sp", "tp"), None),
            P(),
            P(),
            P(),
            P(),
            P(),
            P(("sp", "tp"), None, None),
            P(("sp", "tp"), None, None),
            P(("sp", "tp"), None, None),
            P(("sp", "tp"), None),
            P(("sp", "tp"), None),
        ),
        out_specs=P(("sp", "tp"), None),
        check_vma=False,
    )
```

time: 1210 us -> 317 us (0.26)
  blocking collectives: 874 us -> 114 us
  local copies, waits for them, and re-layouts: 119 us -> 47.8 us
  other arithmetic: 41.6 us -> 1.5 us
  matrix products: 41.6 us -> 28.9 us
    all_to_all x1, blocking collectives: 874 us -> 114 us  [routed_sum(): lax.all_to_all(outgoing, ('sp', 'tp'), split_axis=1, concat_axis=1, tiled...]
    dynamic_update_slice x34 -> x0, local copies, waits for them, and re-layouts: 25.7 us -> none  [the longest x16 13.4 us: add_one(): lax.dynamic_update_index_in_dim(partial_store, partials, shard_step, 0)]
    reduce_sum x2 -> x0, other arithmetic: 21.8 us -> none  [the longest x1 21.6 us: stick_breaking(): return jnp.sum(jnp.exp(later)[..., None] * partials, axis=0)]
    broadcast_in_dim x30 -> x0, local copies, waits for them, and re-layouts: 13 us -> none  [the longest x15 8.94 us: add_one(): lax.dynamic_update_index_in_dim(total_store, totals, shard_step, 0)]
    dot_general x4 -> x0, matrix products: 12.7 us -> none  [the longest x2 11.8 us: block_terms(): jnp.einsum('hqk,khd->qhd', weights, value_block, preferred_element_type=j...]
  transfers between devices with their start and end apart: 3 -> 3, of which waited for: 3 -> 3; matrix products, arithmetic and copies ran while one was open for 0% -> 1% of each run, Pallas kernels for 0% -> 0%
where the time goes in v1:
time: 317 us; the launch traced here: 316 us
  blocking collectives  114 us (36%)
  waiting for transfers between devices  96.9 us (31%)
  local copies, waits for them, and re-layouts  47.8 us (15%)
  matrix products  28.9 us (9%)
  between operations  13.6 us (4%)
  starting transfers between devices  10.7 us (3%)
    all_to_all x1, blocking collectives, routed_sum(): lax.all_to_all(outgoing, ('sp', 'tp'), split_axis=1, concat_axis=1, tiled...  114 us
    all_gather x1, waiting for transfers between devices, attention(): everyone = lax.all_gather(packed, 'sp', axis=0, tiled=False)  52.5 us
    all_to_all x1, waiting for transfers between devices, routed_sum(): lax.all_to_all(result.reshape(arrived.shape), ('sp', 'tp'), split_axis=1,...  39.4 us
    reshape x2, local copies, waits for them, and re-layouts, routed_sum(): outgoing.reshape(local_experts, device_count, capacity, model_width)  17.6 us
    dot_general x1, matrix products, routed_sum(): jnp.einsum('erf,efd->erd', hidden, expert_down, preferred_element_type=jn...  10.3 us
    reshape x1, local copies, waits for them, and re-layouts, routed_sum(): returned.reshape(-1, model_width)  8.83 us
    convert_element_type x1, local copies, waits for them, and re-layouts, routed_sum(): result = jnp.einsum('erf,efd->erd', hidden, expert_down, preferred_elemen...  6.85 us
  transfers between devices with their start and end apart: 3, of which 3 were waited for; matrix products, arithmetic and copies ran while one was open for 1% of the time, Pallas kernels for 0%

profile of v1, /device:TPU:1, one launch (start us, length us, event | category | flops | bytes accessed | tf_op | source)
XLA Modules:
  0.0 315.9 jit_solution(15442460117368569608)
XLA Ops:
  6.5 0.0 copy-start
  6.5 0.0 all-gather.3.cloned.1.call-start
  6.6 1.2 reshape.144
  7.8 0.1 copy.130
  7.9 0.9 copy.143
  8.9 0.7 pad_maximum_fusion
  9.6 0.0 all-gather.3.cloned.1.call-update
  9.6 0.8 copy.133
  10.4 0.1 eq.67
  10.5 0.1 eq.63
  10.6 0.1 copy.135
  10.7 0.2 fusion.20
  11.0 0.1 copy.136
  11.1 0.2 fusion.19
  11.4 0.1 sub.14
  11.5 0.1 copy.137
  11.6 0.0 copy-done.4
  11.6 0.2 copy.131.q_ref
  11.8 0.0 copy-done.6
  11.8 52.5 %all-gather.3.cloned.1.call-done = bf16[16384,128]{1,0:T(8,128)(2,1)} async-done(((bf16[1024,128]{1,0:T(8,128)(2,1)}), bf16[16384,128]{1,0:T(8,128)(2,1)}) %all-gather.3.cloned.1.call-update) | async-done | bytes 4194320 | tf_op jit(solution)/shard_map/all_gather | solution.py:93
  64.3 0.0 copy-done.2
  64.3 2.2 copy-done.1
  66.5 2.8 attention.1
  69.3 0.0 copy-start.5
  69.3 0.8 copy.132
  70.1 5.1 %all-to-all-start = ((bf16[8,128,64]{1,2,0:T(8,128)(2,1)}), bf16[8,128,64]{1,2,0:T(8,128)(2,1)S(1)}, u32[]{:S(2)}, u32[]{:S(2)}) async-start(bf16[8,128,64]{1,2,0:T(8,128)(2,1)} %copy.132), calls=%async_computation | async-start | bytes 262144 | tf_op jit(solution)/shard_map/all_to_all | solution.py:171
  75.2 0.2 fusion.16
  75.5 5.0 %all-to-all-done = bf16[8,128,64]{1,2,0:T(8,128)(2,1)S(1)} async-done(((bf16[8,128,64]{1,2,0:T(8,128)(2,1)}), bf16[8,128,64]{1,2,0:T(8,128)(2,1)S(1)}, u32[]{:S(2)}, u32[]{:S(2)}) %all-to-all-start) | async-done | bytes 131104 | tf_op jit(solution)/shard_map/all_to_all | solution.py:171
  80.5 0.0 copy-done
  80.5 1.6 multiply_reduce_fusion.1
  82.1 0.0 copy-done.5
  82.1 2.7 convolution_convert_fusion.1
  84.8 9.1 %reshape.148 = bf16[2,128,3,2048]{3,2,1,0:T(4,128)(2,1)} reshape(bf16[768,2048]{1,0:T(8,128)(2,1)} %convolution_convert_fusion.1) | data formatting | bytes 6291456 | tf_op jit(solution)/shard_map/reshape | solution.py:134
  93.9 8.5 %copy.138 = bf16[2,128,3,2048]{3,0,2,1:T(2,128)(2,1)S(1)} copy(bf16[2,128,3,2048]{3,2,1,0:T(4,128)(2,1)} %reshape.148) | data formatting | bytes 6291456 | tf_op jit(solution)/shard_map/reshape | solution.py:134
  102.4 0.0 copy-start.7
  102.4 113.7 %all_to_all.29 = bf16[2,128,3,2048]{3,0,2,1:T(2,128)(2,1)S(1)} all-to-all(bf16[2,128,3,2048]{3,0,2,1:T(2,128)(2,1)S(1)} %copy.138), channel_id=1, replica_groups=mesh['sp'=16,'tp'=8] {'sp','tp'}, dimensions={1} | all-to-all | bytes 6291456 | tf_op jit(solution)/shard_map/all_to_all | solution.py:135
  216.1 1.7 copy-done.3
  217.8 3.2 fusion.2
  220.9 10.3 %convolution_convert_fusion = bf16[2,384,2048]{2,1,0:T(8,128)(2,1)} fusion(bf16[2,512,2048]{2,1,0:T(8,128)(2,1)} %param.27, f32[2,384,512]{2,1,0:T(8,128)} %fusion.2, bf16[2,2048,512]{2,1,0:T(8,128)(2,1)} %param.26, bf16[2,384,2048]{2,0,1:T(2,128)(2,1)} %bitcast.48), kind=kOutput, calls=%fused_computation.1 | convolution fusion | flops 3225157632 | bytes 16252928 | tf_op jit(solution)/shard_map/erf,efd->erd/dot_general | solution.py:140
  231.2 6.8 %copy.141 = bf16[2,384,2048]{2,0,1:T(2,128)(2,1)} copy(bf16[2,384,2048]{2,1,0:T(8,128)(2,1)} %convolution_convert_fusion) | data formatting | bytes 6291456 | tf_op jit(solution)/shard_map/convert_element_type | solution.py:142
  238.1 5.6 %all-to-all-start.2 = ((bf16[2,128,3,2048]{3,0,2,1:T(2,128)(2,1)}), bf16[2,128,3,2048]{3,0,2,1:T(2,128)(2,1)}, u32[]{:S(2)}, u32[]{:S(2)}) async-start(bf16[2,128,3,2048]{3,0,2,1:T(2,128)(2,1)} %bitcast.46), calls=%async_computation.2 | async-start | bytes 6291456 | tf_op jit(solution)/shard_map/all_to_all | solution.py:143
  243.7 2.1 fusion.37
  245.8 39.4 %all-to-all-done.2 = bf16[2,128,3,2048]{3,0,2,1:T(2,128)(2,1)} async-done(((bf16[2,128,3,2048]{3,0,2,1:T(2,128)(2,1)}), bf16[2,128,3,2048]{3,0,2,1:T(2,128)(2,1)}, u32[]{:S(2)}, u32[]{:S(2)}) %all-to-all-start.2) | async-done | bytes 3145760 | tf_op jit(solution)/shard_map/all_to_all | solution.py:143
  285.2 6.0 %copy.142 = bf16[2,128,3,2048]{3,2,1,0:T(4,128)(2,1)} copy(bf16[2,128,3,2048]{3,0,2,1:T(2,128)(2,1)} %all-to-all-done.2) | data formatting | bytes 6291456 | tf_op jit(solution)/shard_map/all_to_all | solution.py:143
  291.2 8.8 %reshape.153 = bf16[768,2048,1]{1,0,2:T(8,128)(2,1)} reshape(bf16[2,128,3,2048]{3,2,1,0:T(4,128)(2,1)} %copy.142) | data formatting | bytes 6291456 | tf_op jit(solution)/shard_map/reshape | solution.py:147
  300.0 0.0 copy-done.8
  300.0 4.8 %multiply_reduce_fusion = f32[128,2048]{1,0:T(8,128)} fusion(bf16[768,2048,1]{1,0,2:T(8,128)(2,1)} %reshape.153, f32[128,4]{0,1:T(4,128)S(1)} %copy-done.8, s32[128,4]{0,1:T(4,128)S(1)} %fusion.32), kind=kOutput, calls=%fused_computation | convolution fusion | flops 1612840960 | bytes 4198400 | tf_op jit(solution)/shard_map/dot_general | solution.py:146
  304.8 4.2 %fusion.7 = bf16[128,2048]{1,0:T(8,128)(2,1)} fusion(f32[128,2048]{1,0:T(8,128)} %multiply_reduce_fusion, f32[128,2048]{1,0:T(8,128)S(1)} %get-tuple-element.6, bf16[512,2048]{1,0:T(8,128)(2,1)} %param.24, bf16[2048,512]{1,0:T(8,128)(2,1)} %param.23, f32[128,512]{1,0:T(8,128)S(1)} %fusion.37, f32[2048]{0:T(1024)S(1)} %copy-done.5, f32[128]{0:T(128)S(1)} %add_rsqrt_fusion), kind=kOutput, calls=%fused_computation.12 | convolution fusion | flops 538836992 | bytes 7086592 | tf_op jit(solution)/shard_map/dot_general | solution.py:181
  (17 shorter events, 0.2 us)
Async XLA Ops:
  6.5 73.9 %copy-start = (bf16[512,2048]{1,0:T(8,128)(2,1)S(1)}, bf16[512,2048]{1,0:T(8,128)(2,1)}, u32[]{:S(2)}) copy-start(bf16[512,2048]{1,0:T(8,128)(2,1)} %param.20) | copy-start | bytes 6291460
  6.5 5.2 %copy-start.6 = (s32[128,4]{0,1:T(4,128)S(1)}, s32[128,4]{0,1:T(4,128)}, u32[]{:S(2)}) copy-start(s32[128,4]{0,1:T(4,128)} %param.28) | copy-start | bytes 6148
  6.5 5.0 %copy-start.4 = (bf16[1024,64]{0,1:T(8,128)(2,1)S(1)}, bf16[1024,64]{0,1:T(8,128)(2,1)}, u32[]{:S(2)}) copy-start(bf16[1024,64]{0,1:T(8,128)(2,1)} %param.15) | copy-start | bytes 393220
  6.5 57.7 %copy-start.2 = (f32[64]{0:T(128)S(1)}, f32[64]{0:T(128)}, u32[]{:S(2)}) copy-start(f32[64]{0:T(128)} %param.18) | copy-start | bytes 772
  6.5 57.7 %all-gather.3.cloned.1.call-start = ((), (), s32[]{:S(2)}) async-start(), calls=%async_computation.3 | async-start | bytes 4456448 | tf_op jit(solution)/shard_map/all_gather | solution.py:93
  64.3 2.2 copy-start.1
  69.3 12.8 %copy-start.5 = (f32[2048]{0:T(1024)S(1)}, f32[2048]{0:T(1024)}, u32[]{:S(2)}) copy-start(f32[2048]{0:T(1024)} %param.21) | copy-start | bytes 24580
  70.1 10.4 %all-to-all-start = ((bf16[8,128,64]{1,2,0:T(8,128)(2,1)}), bf16[8,128,64]{1,2,0:T(8,128)(2,1)S(1)}, u32[]{:S(2)}, u32[]{:S(2)}) async-start(bf16[8,128,64]{1,2,0:T(8,128)(2,1)} %copy.132), calls=%async_computation | async-start | bytes 262144 | tf_op jit(solution)/shard_map/all_to_all | solution.py:171
  102.4 115.4 %copy-start.7 = (bf16[2,2048,512]{2,1,0:T(8,128)(2,1)S(1)}, bf16[2,2048,512]{2,1,0:T(8,128)(2,1)}, u32[]{:S(2)}) copy-start(bf16[2,2048,512]{2,1,0:T(8,128)(2,1)} %param.25) | copy-start | bytes 12582916
  216.1 1.7 copy-start.3
  238.1 47.1 %all-to-all-start.2 = ((bf16[2,128,3,2048]{3,0,2,1:T(2,128)(2,1)}), bf16[2,128,3,2048]{3,0,2,1:T(2,128)(2,1)}, u32[]{:S(2)}, u32[]{:S(2)}) async-start(bf16[2,128,3,2048]{3,0,2,1:T(2,128)(2,1)} %bitcast.46), calls=%async_computation.2 | async-start | bytes 6291456 | tf_op jit(solution)/shard_map/all_to_all | solution.py:143
  291.2 8.8 %copy-start.8 = (f32[128,4]{0,1:T(4,128)S(1)}, f32[128,4]{0,1:T(4,128)}, u32[]{:S(2)}) copy-start(f32[128,4]{0,1:T(4,128)} %param.29) | copy-start | bytes 6148
Sparse Core Ops, SparseCore 0:
  9.7 54.5 all-gather.2

commit v2 on v1

--- a/solution.py
+++ b/solution.py
@@ -15,6 +15,7 @@
 
 LOG2E = 1.4426950408889634
 TILE = 256
+MESH = pl.DeviceIdType.MESH
 
 
 def tile_terms(q2, keys, values, tri, carry, mask):
@@ -33,78 +34,248 @@
     return out, carry + jnp.broadcast_to(total, carry.shape)
 
 
-def attention_kernel(q_ref, kv_ref, gain_ref, out_ref, q2_ref, acc_ref, carry_ref, tri_ref):
-    me = lax.axis_index("sp")
+def attention_kernel(
+    q_ref, k_ref, v_ref, gain_ref, out_ref,
+    q_own, q_ref2, key_ref, value_ref, acc_ref, carry_ref, tri_ref, out_own, out_in,
+    q_send, q_recv, q_local, send_sem, key_recv, value_recv, out_send, out_recv, out_local,
+):
+    me, head = lax.axis_index("sp"), lax.axis_index("tp")
+    row, column = me // 4, me % 4
+    half = q_ref.shape[0] // 2
+
     q = q_ref[...].astype(jnp.float32) * (LOG2E / math.sqrt(HEAD_DIM))
     high = q.astype(jnp.bfloat16)
     low = (q - high.astype(jnp.float32)).astype(jnp.bfloat16)
-    q2_ref[...] = jnp.concatenate([high, low], axis=1)
-    row = lax.broadcasted_iota(jnp.int32, (TILE, TILE), 0)
-    column = lax.broadcasted_iota(jnp.int32, (TILE, TILE), 1)
-    tri_ref[...] = (row > column).astype(jnp.float32).astype(jnp.bfloat16)
+    both = jnp.concatenate([high, low], axis=1)
+    q_own[0] = both[:half]
+    q_own[1] = both[half:]
+    for part in range(8):
+        block = k_ref[pl.ds(part * 128, 128), :].astype(jnp.float32)
+        key_ref[me, pl.ds(part * HEAD_DIM, HEAD_DIM), :] = block.T.astype(jnp.bfloat16)
+    v = v_ref[...].astype(jnp.float32)
+    value_ref[me] = jnp.concatenate([v[:half], v[half:]], axis=1).astype(jnp.bfloat16)
+
+    def copy(source, target, out_sem, in_sem, where, which):
+        return pltpu.make_async_remote_copy(
+            src_ref=source, dst_ref=target, send_sem=out_sem, recv_sem=in_sem,
+            device_id=(where, which), device_id_type=MESH,
+        )
+
+    slot = jnp.where(me < 8, 1, 0)
+    for part in range(2):
+        place = 2 * me + part
+        owner = jnp.where(place < 16, place, 31 - place)
+
+        @pl.when(owner != me)
+        def _():
+            copy(q_own.at[part], q_ref2.at[slot], q_send.at[part], q_recv.at[slot], owner, head).start()
+
+        @pl.when(owner == me)
+        def _():
+            pltpu.make_async_copy(q_own.at[part], q_ref2.at[slot], q_local).start()
+
+    steps = (1, 3, 2)
+
+    def key_copy(block, n, where):
+        return copy(key_ref.at[block], key_ref.at[block], send_sem.at[n], key_recv.at[block], where, head)
+
+    def value_copy(block, n, where):
+        return copy(value_ref.at[block], value_ref.at[block], send_sem.at[n], value_recv.at[block], where, head)
+
+    along = [row * 4 + (column + d) % 4 for d in steps]
+    across = [(row + d) % 4 * 4 + column for d in steps]
+    sent = []
+    for n in range(3):
+        sent.append(key_copy(me, n, along[n]))
+        sent.append(value_copy(me, 3 + n, across[n]))
+    for n in range(3):
+        sent.append(key_copy(me, 6 + n, across[n]))
+        sent.append(value_copy(me, 9 + n, along[n]))
+    for one in sent:
+        one.start()
+
+    r = lax.broadcasted_iota(jnp.int32, (TILE, TILE), 0)
+    c = lax.broadcasted_iota(jnp.int32, (TILE, TILE), 1)
+    tri_ref[...] = (r > c).astype(jnp.float32).astype(jnp.bfloat16)
     acc_ref[...] = jnp.zeros_like(acc_ref)
     carry_ref[...] = jnp.zeros_like(carry_ref)
-    tiles = q_ref.shape[0] // TILE
-
-    def chunk(block, part):
-        left = kv_ref[block, pl.ds(part * 128, 64), :]
-        right = kv_ref[block, pl.ds(part * 128 + 64, 64), :]
-        keys = jnp.concatenate([left, right], axis=1)
-        keys = jnp.concatenate([keys, keys], axis=0)
-        values = kv_ref[block, pl.ds(512 + (part % 2) * TILE, TILE), :]
-        side = lax.broadcasted_iota(jnp.int32, values.shape, 1) // HEAD_DIM
-        return keys, jnp.where(side == part // 2, values, jnp.zeros_like(values))
-
-    def add(tile, keys, values, mask):
-        rows = pl.ds(tile * TILE, TILE)
-        out, carry = tile_terms(
-            q2_ref[rows, :], keys, values, tri_ref[...], carry_ref[rows, :], mask
-        )
-        acc_ref[rows, :] += out
-        carry_ref[rows, :] = carry
-
-    for part in range(tiles - 1, -1, -1):
-        keys, values = chunk(me, part)
-        for tile in range(part, tiles):
-            add(tile, keys, values, column < row if tile == part else None)
-
-    def step(i, unused):
-        keys, values = chunk(me - 1 - i // tiles, tiles - 1 - i % tiles)
-        for tile in range(tiles):
-            add(tile, keys, values, None)
+
+    for n in range(3):
+        key_copy(along[n], 0, me).wait_recv()
+        for m in range(3):
+            one = key_copy(along[n], 12 + 3 * n + m, across[m])
+            one.start()
+            sent.append(one)
+        value_copy(across[n], 0, me).wait_recv()
+        for m in range(3):
+            one = value_copy(across[n], 21 + 3 * n + m, along[m])
+            one.start()
+            sent.append(one)
+
+    def arrived(block):
+        @pl.when(block // 4 != row)
+        def _():
+            key_copy(block, 0, me).wait_recv()
+
+        @pl.when(block % 4 != column)
+        def _():
+            value_copy(block, 0, me).wait_recv()
+
+    def unit(which, place, diagonal):
+        block, side = place // 2, place % 2
+        for part in (1, 0):
+            at = (2 * side + part) * 128
+            left = key_ref[block, pl.ds(at, HEAD_DIM), :]
+            right = key_ref[block, pl.ds(at + HEAD_DIM, HEAD_DIM), :]
+            keys = jnp.concatenate([left, right], axis=1)
+            keys = jnp.concatenate([keys, keys], axis=0)
+            values = value_ref[block, pl.ds(part * TILE, TILE), :]
+            lanes = lax.broadcasted_iota(jnp.int32, values.shape, 1) // HEAD_DIM
+            values = jnp.where(lanes == side, values, jnp.zeros_like(values))
+            for tile in range(2):
+                if diagonal and tile < part:
+                    continue
+                rows = pl.ds(tile * TILE, TILE)
+                mask = c < r if diagonal and tile == part else None
+                out, carry = tile_terms(
+                    q_ref2[which, rows, :], keys, values, tri_ref[...], carry_ref[which, rows, :], mask
+                )
+                acc_ref[which, rows, :] += out
+                carry_ref[which, rows, :] = carry
+
+    def finish(which, place):
+        acc = acc_ref[which]
+        mixed = acc[:, :HEAD_DIM] + acc[:, HEAD_DIM:]
+        inverse = lax.rsqrt(jnp.mean(mixed * mixed, axis=1, keepdims=True) + EPSILON)
+        normed = mixed * inverse * gain_ref[...]
+        for piece in range(4):
+            at = piece * 128
+            two = jnp.concatenate([normed[at : at + 64], normed[at + 64 : at + 128]], axis=1)
+            out_own[4 * which + piece] = two.astype(jnp.bfloat16)
+        for piece in range(4):
+            n = 4 * which + piece
+            where, token = place // 2, (place % 2) * 4 + piece
+            mine = (where == me) & (token == head)
+
+            @pl.when(jnp.logical_not(mine))
+            def _():
+                copy(out_own.at[n], out_in.at[head], out_send.at[n], out_recv.at[head], where, token).start()
+
+            @pl.when(mine)
+            def _():
+                pltpu.make_async_copy(out_own.at[n], out_in.at[head], out_local).start()
+
+    @pl.when(me != 10)
+    def _():
+        copy(q_own.at[0], q_ref2.at[0], q_send.at[0], q_recv.at[0], me, head).wait_recv()
+
+    @pl.when(me != 0)
+    def _():
+        copy(q_own.at[0], q_ref2.at[1], q_send.at[0], q_recv.at[1], me, head).wait_recv()
+
+    @pl.when((me == 0) | (me == 10))
+    def _():
+        pltpu.make_async_copy(q_own.at[0], q_ref2.at[0], q_local).wait()
+
+    far = 31 - me
+    arrived(far // 2)
+    unit(0, far, True)
+
+    def far_step(n, unused):
+        place = far - 1 - n
+
+        @pl.when(place % 2 == 1)
+        def _():
+            arrived(place // 2)
+
+        unit(0, place, False)
         return unused
 
-    lax.fori_loop(0, me * tiles, step, 0)
-    mixed = acc_ref[:, :HEAD_DIM] + acc_ref[:, HEAD_DIM:]
-    inverse = lax.rsqrt(jnp.mean(mixed * mixed, axis=1, keepdims=True) + EPSILON)
-    out_ref[...] = (mixed * inverse * gain_ref[...]).astype(jnp.bfloat16)
-
-
-def pack_keys_values(key_heads, value_heads):
-    rows = key_heads.shape[0]
-    keys = key_heads.reshape(rows // 128, 128, HEAD_DIM).transpose(0, 2, 1).reshape(-1, 128)
-    values = value_heads.reshape(2, rows // 2, HEAD_DIM).transpose(1, 0, 2).reshape(-1, 128)
-    return jnp.concatenate([keys, values], axis=0)
+    lax.fori_loop(0, far, far_step, 0)
+    finish(0, far)
+    unit(1, me, True)
+
+    def near_step(n, unused):
+        unit(1, me - 1 - n, False)
+        return unused
+
+    lax.fori_loop(0, me, near_step, 0)
+    finish(1, me)
+
+    def drain(n, unused):
+        arrived(n)
+        return unused
+
+    lax.fori_loop(far // 2 + 1, 16, drain, 0)
+    for part in range(2):
+        place = 2 * me + part
+        owner = jnp.where(place < 16, place, 31 - place)
+
+        @pl.when(owner != me)
+        def _():
+            copy(q_own.at[part], q_ref2.at[slot], q_send.at[part], q_recv.at[slot], owner, head).wait_send()
+    for one in sent:
+        one.wait_send()
+
+    place = 2 * me + head // 4
+    owner = jnp.where(place < 16, place, 31 - place)
+    for other in range(8):
+        @pl.when(jnp.logical_not((owner == me) & (other == head)))
+        def _():
+            copy(out_own.at[0], out_in.at[other], out_send.at[0], out_recv.at[other], me, head).wait_recv()
+    for which, spot in ((0, far), (1, me)):
+        for piece in range(4):
+            n = 4 * which + piece
+            where, token = spot // 2, (spot % 2) * 4 + piece
+            mine = (where == me) & (token == head)
+
+            @pl.when(jnp.logical_not(mine))
+            def _():
+                copy(out_own.at[n], out_in.at[head], out_send.at[n], out_recv.at[head], where, token).wait_send()
+
+            @pl.when(mine)
+            def _():
+                pltpu.make_async_copy(out_own.at[n], out_in.at[head], out_local).wait()
+
+    for pair in range(4):
+        one = out_in[2 * pair].astype(jnp.float32)
+        two = out_in[2 * pair + 1].astype(jnp.float32)
+        one = jnp.concatenate([one[:, :HEAD_DIM], one[:, HEAD_DIM:]], axis=0)
+        two = jnp.concatenate([two[:, :HEAD_DIM], two[:, HEAD_DIM:]], axis=0)
+        out_ref[:, pl.ds(pair * 128, 128)] = jnp.concatenate([one, two], axis=1).astype(jnp.bfloat16)
 
 
 def attention(queries, key_heads, value_heads, head_gain):
     rows = queries.shape[0]
-    packed = pack_keys_values(key_heads, value_heads)
-    everyone = lax.all_gather(packed, "sp", axis=0, tiled=False)
+    half = rows // 2
     return pl.pallas_call(
         attention_kernel,
-        out_shape=jax.ShapeDtypeStruct((rows, HEAD_DIM), jnp.bfloat16),
-        in_specs=[pl.BlockSpec(memory_space=pltpu.VMEM)] * 3,
+        out_shape=jax.ShapeDtypeStruct((128, 8 * HEAD_DIM), jnp.bfloat16),
+        in_specs=[pl.BlockSpec(memory_space=pltpu.VMEM)] * 4,
         out_specs=pl.BlockSpec(memory_space=pltpu.VMEM),
         scratch_shapes=[
-            pltpu.VMEM((rows, 128), jnp.bfloat16),
-            pltpu.VMEM((rows, 128), jnp.float32),
-            pltpu.VMEM((rows, 128), jnp.float32),
+            pltpu.VMEM((2, half, 128), jnp.bfloat16),
+            pltpu.VMEM((2, half, 128), jnp.bfloat16),
+            pltpu.VMEM((16, half, 128), jnp.bfloat16),
+            pltpu.VMEM((16, half, 128), jnp.bfloat16),
+            pltpu.VMEM((2, half, 128), jnp.float32),
+            pltpu.VMEM((2, half, 128), jnp.float32),
             pltpu.VMEM((TILE, TILE), jnp.bfloat16),
+            pltpu.VMEM((8, 64, 128), jnp.bfloat16),
+            pltpu.VMEM((8, 64, 128), jnp.bfloat16),
+            pltpu.SemaphoreType.DMA((2,)),
+            pltpu.SemaphoreType.DMA((2,)),
+            pltpu.SemaphoreType.DMA,
+            pltpu.SemaphoreType.DMA((30,)),
+            pltpu.SemaphoreType.DMA((16,)),
+            pltpu.SemaphoreType.DMA((16,)),
+            pltpu.SemaphoreType.DMA((8,)),
+            pltpu.SemaphoreType.DMA((8,)),
+            pltpu.SemaphoreType.DMA,
         ],
-        compiler_params=pltpu.CompilerParams(vmem_limit_bytes=40 << 20),
+        compiler_params=pltpu.CompilerParams(vmem_limit_bytes=40 << 20, has_side_effects=True),
         name="attention",
-    )(queries, everyone, head_gain.reshape(1, HEAD_DIM))
+    )(queries, key_heads, value_heads, head_gain.reshape(1, HEAD_DIM))
 
 
 def routed_sum(expert_input, expert_gate, expert_up, expert_down, routed_experts, route_weights):
@@ -167,8 +338,7 @@
     routed_experts,
     route_weights,
 ):
-    head_output = attention(queries, key_heads, value_heads, head_gain)
-    token_heads = lax.all_to_all(head_output, "tp", split_axis=0, concat_axis=1, tiled=True)
+    token_heads = attention(queries, key_heads, value_heads, head_gain)
     branch = jnp.dot(token_heads, out_weight, preferred_element_type=jnp.float32)
     stream = (residual.astype(jnp.float32) + branch).astype(jnp.bfloat16)
     stream_wide = stream.astype(jnp.float32)

time: 317 us -> 255 us (0.80)
  Pallas kernels: 2.82 us -> 84.9 us
  blocking collectives: 114 us -> 51.1 us
  waiting for transfers between devices: 96.9 us -> 39.4 us
  between operations: 13.6 us -> 0.21 us
  starting transfers between devices: 10.7 us -> 5.38 us
  local copies, waits for them, and re-layouts: 47.8 us -> 43.1 us
    pallas_call x1, Pallas kernels: 2.82 us -> 84.9 us  [attention(): pl.pallas_call(attention_kernel, out_shape=jax.ShapeDtypeStruct((128, 8 *...]
    all_to_all x1, blocking collectives: 114 us -> 51.1 us  [routed_sum(): lax.all_to_all(outgoing, ('sp', 'tp'), split_axis=1, concat_axis=1, tiled...]
    all_gather x1 -> x0, waiting for transfers between devices: 52.5 us -> none  [attention(): everyone = lax.all_gather(packed, 'sp', axis=0, tiled=False)]
    all_to_all x1 -> x0, starting transfers between devices: 5.13 us -> none  [body(): lax.all_to_all(head_output, 'tp', split_axis=0, concat_axis=1, tiled=True)]
    all_to_all x1 -> x0, waiting for transfers between devices: 4.99 us -> none  [body(): lax.all_to_all(head_output, 'tp', split_axis=0, concat_axis=1, tiled=True)]
  transfers between devices with their start and end apart: 3 -> 1, of which waited for: 3 -> 1; matrix products, arithmetic and copies ran while one was open for 1% -> 1% of each run, Pallas kernels for 0% -> 0%
where the time goes in v2:
time: 255 us; the launch traced here: 254 us
  Pallas kernels  84.9 us (33%)
  blocking collectives  51.1 us (20%)
  local copies, waits for them, and re-layouts  43.1 us (17%)
  waiting for transfers between devices  39.4 us (15%)
  matrix products  29.1 us (11%)
  starting transfers between devices  5.38 us (2%)
    pallas_call x1, Pallas kernels, attention(): pl.pallas_call(attention_kernel, out_shape=jax.ShapeDtypeStruct((128, 8 *...  84.9 us
    all_to_all x1, blocking collectives, routed_sum(): lax.all_to_all(outgoing, ('sp', 'tp'), split_axis=1, concat_axis=1, tiled...  51.1 us
    all_to_all x1, waiting for transfers between devices, routed_sum(): lax.all_to_all(result.reshape(arrived.shape), ('sp', 'tp'), split_axis=1,...  39.4 us
    reshape x2, local copies, waits for them, and re-layouts, routed_sum(): outgoing.reshape(local_experts, device_count, capacity, model_width)  17.6 us
    dot_general x1, matrix products, routed_sum(): jnp.einsum('erf,efd->erd', hidden, expert_down, preferred_element_type=jn...  10.3 us
    reshape x1, local copies, waits for them, and re-layouts, routed_sum(): returned.reshape(-1, model_width)  8.83 us
    convert_element_type x1, local copies, waits for them, and re-layouts, routed_sum(): result = jnp.einsum('erf,efd->erd', hidden, expert_down, preferred_elemen...  6.85 us
    all_to_all x1, local copies, waits for them, and re-layouts, routed_sum(): lax.all_to_all(result.reshape(arrived.shape), ('sp', 'tp'), split_axis=1,...  6.03 us
  transfers between devices with their start and end apart: 1, of which 1 were waited for; matrix products, arithmetic and copies ran while one was open for 1% of the time, Pallas kernels for 0%

profile of v2, /device:TPU:1, one launch (start us, length us, event | category | flops | bytes accessed | tf_op | source)
XLA Modules:
  0.0 253.9 jit_solution(8488683981924459150)
XLA Ops:
  0.0 0.0 copy-start
  0.0 0.0 copy-start.7
  0.0 0.0 copy-start.3
  0.0 0.0 copy-start.4
  0.0 0.0 copy-start.5
  0.0 0.0 copy-start.1
  0.0 0.9 copy.83
  1.0 0.1 eq.67
  1.1 0.1 eq.63
  1.2 0.1 copy.85
  1.3 0.2 fusion.20
  1.6 0.1 copy.86
  1.7 0.2 fusion.19
  2.0 0.0 copy-start.6
  2.0 0.1 sub.14
  2.1 0.1 copy.87
  2.2 0.0 copy-done.7
  2.2 0.2 fusion.16
  2.4 0.0 copy-done.3
  2.5 0.2 copy.80.q_ref
  2.6 0.0 copy-done.4
  2.6 0.2 copy.81.k_ref
  2.8 0.0 copy-done.5
  2.8 0.2 copy.82.v_ref
  3.0 0.0 copy-done.1
  3.0 84.9 %attention.1 = bf16[128,512]{1,0:T(8,128)(2,1)S(1)} custom-call(bf16[1024,64]{1,0:T(8,128)(2,1)S(1)} %copy.80.q_ref, bf16[1024,64]{1,0:T(8,128)(2,1)S(1)} %copy.81.k_ref, bf16[1024,64]{1,0:T(8,128)(2,1)S(1)} %copy.82.v_ref, f32[1,64]{1,0:T(1,128)S(1)} %bitcast.27), custom_call_target="tpu_custom_call" | custom-call | tf_op jit(solution)/shard_map/attention/pallas_call | solution.py:251
  88.0 0.0 copy-done
  88.0 1.6 multiply_reduce_fusion.1
  89.6 0.0 copy-done.6
  89.6 2.7 %convolution_convert_fusion.1 = bf16[768,2048]{1,0:T(8,128)(2,1)} fusion(bf16[128,768]{1,0:T(8,128)(2,1)S(1)} %fusion.16, f32[128,2048]{1,0:T(8,128)S(1)} %get-tuple-element.6, f32[2048]{0:T(1024)S(1)} %copy-done.6, f32[128]{0:T(128)S(1)} %add_rsqrt_fusion), kind=kOutput, calls=%fused_computation.2 | convolution fusion | flops 405012480 | bytes 4399616 | tf_op jit(solution)/shard_map/rs,rd->sd/dot_general | solution.py:302
  92.4 9.1 %reshape.129 = bf16[2,128,3,2048]{3,2,1,0:T(4,128)(2,1)} reshape(bf16[768,2048]{1,0:T(8,128)(2,1)} %convolution_convert_fusion.1) | data formatting | bytes 6291456 | tf_op jit(solution)/shard_map/reshape | solution.py:305
  101.5 8.5 %copy.88 = bf16[2,128,3,2048]{3,0,2,1:T(2,128)(2,1)S(1)} copy(bf16[2,128,3,2048]{3,2,1,0:T(4,128)(2,1)} %reshape.129) | data formatting | bytes 6291456 | tf_op jit(solution)/shard_map/reshape | solution.py:305
  109.9 0.0 copy-start.8
  109.9 51.1 %all_to_all.10 = bf16[2,128,3,2048]{3,0,2,1:T(2,128)(2,1)S(1)} all-to-all(bf16[2,128,3,2048]{3,0,2,1:T(2,128)(2,1)S(1)} %copy.88), channel_id=1, replica_groups=mesh['sp'=16,'tp'=8] {'sp','tp'}, dimensions={1} | all-to-all | bytes 6291456 | tf_op jit(solution)/shard_map/all_to_all | solution.py:306
  161.0 0.0 copy-start.2
  161.0 1.7 copy-done.2
  162.7 0.0 copy-done.8
  162.7 3.3 %fusion.2 = f32[2,384,512]{2,1,0:T(8,128)} fusion(bf16[2,2048,512]{2,1,0:T(8,128)(2,1)S(1)} %copy-done.8, bf16[2,384,2048]{2,0,1:T(2,128)(2,1)S(1)} %bitcast.29), kind=kOutput, calls=%fused_computation.5 | convolution fusion | flops 1610612736 | bytes 8912896 | tf_op jit(solution)/shard_map/erd,edf->erf/dot_general | solution.py:308
  166.0 10.3 %convolution_convert_fusion = bf16[2,384,2048]{2,1,0:T(8,128)(2,1)} fusion(bf16[2,512,2048]{2,1,0:T(8,128)(2,1)} %param.27, f32[2,384,512]{2,1,0:T(8,128)} %fusion.2, bf16[2,2048,512]{2,1,0:T(8,128)(2,1)} %param.26, bf16[2,384,2048]{2,0,1:T(2,128)(2,1)} %bitcast.30), kind=kOutput, calls=%fused_computation.1 | convolution fusion | flops 3225157632 | bytes 16252928 | tf_op jit(solution)/shard_map/erf,efd->erd/dot_general | solution.py:311
  176.3 6.8 %copy.91 = bf16[2,384,2048]{2,0,1:T(2,128)(2,1)} copy(bf16[2,384,2048]{2,1,0:T(8,128)(2,1)} %convolution_convert_fusion) | data formatting | bytes 6291456 | tf_op jit(solution)/shard_map/convert_element_type | solution.py:313
  183.2 5.4 %all-to-all-start.1 = ((bf16[2,128,3,2048]{3,0,2,1:T(2,128)(2,1)}), bf16[2,128,3,2048]{3,0,2,1:T(2,128)(2,1)}, u32[]{:S(2)}, u32[]{:S(2)}) async-start(bf16[2,128,3,2048]{3,0,2,1:T(2,128)(2,1)} %bitcast.28), calls=%async_computation.1 | async-start | bytes 6291456 | tf_op jit(solution)/shard_map/all_to_all | solution.py:314
  188.6 2.1 fusion.37
  190.7 39.4 %all-to-all-done.1 = bf16[2,128,3,2048]{3,0,2,1:T(2,128)(2,1)} async-done(((bf16[2,128,3,2048]{3,0,2,1:T(2,128)(2,1)}), bf16[2,128,3,2048]{3,0,2,1:T(2,128)(2,1)}, u32[]{:S(2)}, u32[]{:S(2)}) %all-to-all-start.1) | async-done | bytes 3145760 | tf_op jit(solution)/shard_map/all_to_all | solution.py:314
  230.0 6.0 %copy.92 = bf16[2,128,3,2048]{3,2,1,0:T(4,128)(2,1)} copy(bf16[2,128,3,2048]{3,0,2,1:T(2,128)(2,1)} %all-to-all-done.1) | data formatting | bytes 6291456 | tf_op jit(solution)/shard_map/all_to_all | solution.py:314
  236.1 8.8 %reshape.133 = bf16[768,2048,1]{1,0,2:T(8,128)(2,1)} reshape(bf16[2,128,3,2048]{3,2,1,0:T(4,128)(2,1)} %copy.92) | data formatting | bytes 6291456 | tf_op jit(solution)/shard_map/reshape | solution.py:318
  244.9 0.0 copy-done.9
  244.9 4.8 %multiply_reduce_fusion = f32[128,2048]{1,0:T(8,128)} fusion(bf16[768,2048,1]{1,0,2:T(8,128)(2,1)} %reshape.133, f32[128,4]{0,1:T(4,128)S(1)} %copy-done.9, s32[128,4]{0,1:T(4,128)S(1)} %fusion.32), kind=kOutput, calls=%fused_computation | convolution fusion | flops 1612840960 | bytes 4198400 | tf_op jit(solution)/shard_map/dot_general | solution.py:317
  249.7 4.2 %fusion.7 = bf16[128,2048]{1,0:T(8,128)(2,1)} fusion(f32[128,2048]{1,0:T(8,128)} %multiply_reduce_fusion, f32[128,2048]{1,0:T(8,128)S(1)} %get-tuple-element.6, bf16[512,2048]{1,0:T(8,128)(2,1)} %param.24, bf16[2048,512]{1,0:T(8,128)(2,1)} %param.23, f32[128,512]{1,0:T(8,128)S(1)} %fusion.37, f32[2048]{0:T(1024)S(1)} %copy-done.6, f32[128]{0:T(128)S(1)} %add_rsqrt_fusion), kind=kOutput, calls=%fused_computation.12 | convolution fusion | flops 538836992 | bytes 7086592 | tf_op jit(solution)/shard_map/dot_general | solution.py:351
  (9 shorter events, 0.1 us)
Async XLA Ops:
  0.0 88.0 %copy-start = (bf16[512,2048]{1,0:T(8,128)(2,1)S(1)}, bf16[512,2048]{1,0:T(8,128)(2,1)}, u32[]{:S(2)}) copy-start(bf16[512,2048]{1,0:T(8,128)(2,1)} %param.20) | copy-start | bytes 6291460
  0.0 2.2 copy-start.7
  0.0 2.4 copy-start.3
  0.0 2.6 %copy-start.4 = (bf16[1024,64]{0,1:T(8,128)(2,1)S(1)}, bf16[1024,64]{0,1:T(8,128)(2,1)}, u32[]{:S(2)}) copy-start(bf16[1024,64]{0,1:T(8,128)(2,1)} %param.16) | copy-start | bytes 393220
  0.0 2.8 %copy-start.5 = (bf16[1024,64]{0,1:T(8,128)(2,1)S(1)}, bf16[1024,64]{0,1:T(8,128)(2,1)}, u32[]{:S(2)}) copy-start(bf16[1024,64]{0,1:T(8,128)(2,1)} %param.17) | copy-start | bytes 393220
  0.0 3.0 %copy-start.1 = (f32[64]{0:T(128)S(1)}, f32[64]{0:T(128)}, u32[]{:S(2)}) copy-start(f32[64]{0:T(128)} %param.18) | copy-start | bytes 772
  2.0 87.7 %copy-start.6 = (f32[2048]{0:T(1024)S(1)}, f32[2048]{0:T(1024)}, u32[]{:S(2)}) copy-start(f32[2048]{0:T(1024)} %param.21) | copy-start | bytes 24580
  109.9 52.8 %copy-start.8 = (bf16[2,2048,512]{2,1,0:T(8,128)(2,1)S(1)}, bf16[2,2048,512]{2,1,0:T(8,128)(2,1)}, u32[]{:S(2)}) copy-start(bf16[2,2048,512]{2,1,0:T(8,128)(2,1)} %param.25) | copy-start | bytes 12582916
  161.0 1.7 copy-start.2
  183.2 46.9 %all-to-all-start.1 = ((bf16[2,128,3,2048]{3,0,2,1:T(2,128)(2,1)}), bf16[2,128,3,2048]{3,0,2,1:T(2,128)(2,1)}, u32[]{:S(2)}, u32[]{:S(2)}) async-start(bf16[2,128,3,2048]{3,0,2,1:T(2,128)(2,1)} %bitcast.28), calls=%async_computation.1 | async-start | bytes 6291456 | tf_op jit(solution)/shard_map/all_to_all | solution.py:314
  236.1 8.8 %copy-start.9 = (f32[128,4]{0,1:T(4,128)S(1)}, f32[128,4]{0,1:T(4,128)}, u32[]{:S(2)}) copy-start(f32[128,4]{0,1:T(4,128)} %param.29) | copy-start | bytes 6148

commit v3 on v2

--- a/solution.py
+++ b/solution.py
@@ -36,7 +36,7 @@
 
 def attention_kernel(
     q_ref, k_ref, v_ref, gain_ref, out_ref,
-    q_own, q_ref2, key_ref, value_ref, acc_ref, carry_ref, tri_ref, out_own, out_in,
+    q_own, q_ref2, key_ref, value_ref, acc_ref, carry_ref, sum_ref, past_ref, tri_ref, out_own, out_in,
     q_send, q_recv, q_local, send_sem, key_recv, value_recv, out_send, out_recv, out_local,
 ):
     me, head = lax.axis_index("sp"), lax.axis_index("tp")
@@ -97,20 +97,21 @@
     r = lax.broadcasted_iota(jnp.int32, (TILE, TILE), 0)
     c = lax.broadcasted_iota(jnp.int32, (TILE, TILE), 1)
     tri_ref[...] = (r > c).astype(jnp.float32).astype(jnp.bfloat16)
-    acc_ref[...] = jnp.zeros_like(acc_ref)
-    carry_ref[...] = jnp.zeros_like(carry_ref)
+    passed = []
+
+    def forward():
+        for n in range(3):
+            key_copy(along[n], 0, me).wait_recv()
+            for m in range(3):
+                key_copy(along[n], 12 + 3 * n + m, across[m]).start()
+            value_copy(across[n], 0, me).wait_recv()
+            for m in range(3):
+                value_copy(across[n], 21 + 3 * n + m, along[m]).start()
 
     for n in range(3):
-        key_copy(along[n], 0, me).wait_recv()
         for m in range(3):
-            one = key_copy(along[n], 12 + 3 * n + m, across[m])
-            one.start()
-            sent.append(one)
-        value_copy(across[n], 0, me).wait_recv()
-        for m in range(3):
-            one = value_copy(across[n], 21 + 3 * n + m, along[m])
-            one.start()
-            sent.append(one)
+            passed.append(key_copy(along[n], 12 + 3 * n + m, across[m]))
+            passed.append(value_copy(across[n], 21 + 3 * n + m, along[m]))
 
     def arrived(block):
         @pl.when(block // 4 != row)
@@ -138,13 +139,24 @@
                 rows = pl.ds(tile * TILE, TILE)
                 mask = c < r if diagonal and tile == part else None
                 out, carry = tile_terms(
-                    q_ref2[which, rows, :], keys, values, tri_ref[...], carry_ref[which, rows, :], mask
+                    q_ref2[which, rows, :], keys, values, tri_ref[...], carry_ref[which, block, rows, :], mask
                 )
-                acc_ref[which, rows, :] += out
-                carry_ref[which, rows, :] = carry
+                acc_ref[which, block, rows, :] += out
+                carry_ref[which, block, rows, :] = carry
 
     def finish(which, place):
-        acc = acc_ref[which]
+        blank = jnp.zeros((half, 128), jnp.float32)
+        sum_ref[...] = blank
+        past_ref[...] = blank
+
+        def later(n, unused):
+            block = place // 2 - n
+            sum_ref[...] += jnp.exp2(-past_ref[...]) * acc_ref[which, block]
+            past_ref[...] += carry_ref[which, block]
+            return unused
+
+        lax.fori_loop(0, place // 2 + 1, later, 0)
+        acc = sum_ref[...]
         mixed = acc[:, :HEAD_DIM] + acc[:, HEAD_DIM:]
         inverse = lax.rsqrt(jnp.mean(mixed * mixed, axis=1, keepdims=True) + EPSILON)
         normed = mixed * inverse * gain_ref[...]
@@ -178,32 +190,57 @@
         pltpu.make_async_copy(q_own.at[0], q_ref2.at[0], q_local).wait()
 
     far = 31 - me
-    arrived(far // 2)
-    unit(0, far, True)
-
-    def far_step(n, unused):
-        place = far - 1 - n
-
-        @pl.when(place % 2 == 1)
-        def _():
-            arrived(place // 2)
-
-        unit(0, place, False)
+    order = ((0, 0), (0, 1), (1, 0), (0, 3), (3, 0), (0, 2), (2, 0), (1, 1), (3, 3), (1, 3), (3, 1), (1, 2), (2, 1), (3, 2), (2, 3), (2, 2))
+
+    def pick(n, axis):
+        return sum(jnp.where(n == k, one[axis], 0) for k, one in enumerate(order))
+
+    def visit(n, unused):
+        block = (row + pick(n, 0)) % 4 * 4 + (column + pick(n, 1)) % 4
+
+        @pl.when(n == 1)
+        def _():
+            forward()
+
+        @pl.when((block <= far // 2) & (n > 0))
+        def _():
+            arrived(block)
+
+        def pair(i, unused):
+            which, side = i // 2, 1 - i % 2
+            top = jnp.where(which == 0, far, me)
+            place = 2 * block + side
+
+            @pl.when((side == 1) & (2 * block <= top))
+            def _():
+                acc_ref[which, block] = jnp.zeros((half, 128), jnp.float32)
+                carry_ref[which, block] = jnp.zeros((half, 128), jnp.float32)
+
+            @pl.when(place < top)
+            def _():
+                unit(which, place, False)
+
+            @pl.when(place == top)
+            def _():
+                unit(which, place, True)
+
+            return unused
+
+        @pl.when(block <= far // 2)
+        def _():
+            lax.fori_loop(0, 4, pair, 0)
+
         return unused
 
-    lax.fori_loop(0, far, far_step, 0)
+    lax.fori_loop(0, 16, visit, 0)
     finish(0, far)
-    unit(1, me, True)
-
-    def near_step(n, unused):
-        unit(1, me - 1 - n, False)
-        return unused
-
-    lax.fori_loop(0, me, near_step, 0)
     finish(1, me)
 
     def drain(n, unused):
-        arrived(n)
+        @pl.when(n != me)
+        def _():
+            arrived(n)
+
         return unused
 
     lax.fori_loop(far // 2 + 1, 16, drain, 0)
@@ -214,7 +251,7 @@
         @pl.when(owner != me)
         def _():
             copy(q_own.at[part], q_ref2.at[slot], q_send.at[part], q_recv.at[slot], owner, head).wait_send()
-    for one in sent:
+    for one in sent + passed:
         one.wait_send()
 
     place = 2 * me + head // 4
@@ -258,8 +295,10 @@
             pltpu.VMEM((2, half, 128), jnp.bfloat16),
             pltpu.VMEM((16, half, 128), jnp.bfloat16),
             pltpu.VMEM((16, half, 128), jnp.bfloat16),
-            pltpu.VMEM((2, half, 128), jnp.float32),
-            pltpu.VMEM((2, half, 128), jnp.float32),
+            pltpu.VMEM((2, 16, half, 128), jnp.float32),
+            pltpu.VMEM((2, 16, half, 128), jnp.float32),
+            pltpu.VMEM((half, 128), jnp.float32),
+            pltpu.VMEM((half, 128), jnp.float32),
             pltpu.VMEM((TILE, TILE), jnp.bfloat16),
             pltpu.VMEM((8, 64, 128), jnp.bfloat16),
             pltpu.VMEM((8, 64, 128), jnp.bfloat16),
@@ -278,47 +317,232 @@
     )(queries, key_heads, value_heads, head_gain.reshape(1, HEAD_DIM))
 
 
-def routed_sum(expert_input, expert_gate, expert_up, expert_down, routed_experts, route_weights):
-    row_count, pick_count = routed_experts.shape
-    local_experts = expert_gate.shape[0]
-    model_width = expert_input.shape[1]
-    sp_count = lax.axis_size("sp")
-    tp_count = lax.axis_size("tp")
-    device_count = sp_count * tp_count
-    expert_count = local_experts * device_count
-    capacity = max(2, 3 * row_count * pick_count // (2 * expert_count))
-    flat_experts = routed_experts.reshape(-1)
-    expert_table = (
-        flat_experts[:, None] == jnp.arange(expert_count, dtype=jnp.int32)[None, :]
-    ).astype(jnp.int32)
-    ranking = jnp.sum(jnp.cumsum(expert_table, axis=0) * expert_table, axis=1) - 1
-    holder = flat_experts // local_experts
-    resident = flat_experts % local_experts
-    slot_index = (resident * device_count + holder) * capacity + ranking
-    placement = (
-        slot_index[:, None] == jnp.arange(expert_count * capacity, dtype=jnp.int32)[None, :]
-    ).astype(jnp.bfloat16)
-    token_place = jnp.sum(placement.reshape(row_count, pick_count, -1), axis=1)
-    outgoing = jnp.einsum(
-        "rs,rd->sd", token_place, expert_input, preferred_element_type=jnp.float32
-    ).astype(jnp.bfloat16)
-    outgoing = outgoing.reshape(local_experts, device_count, capacity, model_width)
-    arrived = lax.all_to_all(outgoing, ("sp", "tp"), split_axis=1, concat_axis=1, tiled=True)
-    grouped = arrived.reshape(local_experts, -1, model_width)
-    gate_part = jnp.einsum("erd,edf->erf", grouped, expert_gate, preferred_element_type=jnp.float32)
-    up_part = jnp.einsum("erd,edf->erf", grouped, expert_up, preferred_element_type=jnp.float32)
-    hidden = (jax.nn.silu(gate_part) * up_part).astype(jnp.bfloat16)
-    result = jnp.einsum(
-        "erf,efd->erd", hidden, expert_down, preferred_element_type=jnp.float32
-    ).astype(jnp.bfloat16)
-    returned = lax.all_to_all(
-        result.reshape(arrived.shape), ("sp", "tp"), split_axis=1, concat_axis=1, tiled=True
+def mixture_kernel(
+    head_ref, residual_ref, gain_ref, expert_ref, route_ref,
+    out_weight, shared_gate, shared_up, shared_down, expert_gate, expert_up, expert_down,
+    final_ref,
+    ow_ref, sg_ref, su_ref, sd_ref, eg_ref, eu_ref, ed_ref,
+    stream_ref, x_ref, place_ref, mix_ref, stage_ref, outgoing, arrived, rows_ref, hidden_ref,
+    result, returned, total_ref,
+    load_sem, out_send, out_recv, back_send, back_recv, local_sem,
+):
+    me = lax.axis_index("sp") * 8 + lax.axis_index("tp")
+    tokens, width = residual_ref.shape
+    devices, slots = 128, 3
+    chunks = width // 128
+    hidden = sg_ref.shape[1]
+    f32, bf16 = jnp.float32, jnp.bfloat16
+
+    loads = [
+        pltpu.make_async_copy(source, target, load_sem.at[n])
+        for n, (source, target) in enumerate(
+            (
+                (out_weight, ow_ref), (shared_gate, sg_ref), (shared_up, su_ref), (shared_down, sd_ref),
+                (expert_gate, eg_ref), (expert_up, eu_ref), (expert_down, ed_ref),
+            )
+        )
+    ]
+    for one in loads:
+        one.start()
+
+    line = lax.broadcasted_iota(jnp.int32, (2 * devices, tokens), 0)
+    expert = 2 * (line % devices) + line // devices
+    named = jnp.zeros((2 * devices, tokens), f32)
+    weight = jnp.zeros((2 * devices, tokens), f32)
+    for pick in range(expert_ref.shape[0]):
+        hit = expert_ref[pick : pick + 1, :] == expert
+        named = named + jnp.where(hit, 1.0, 0.0)
+        weight = weight + jnp.where(hit, route_ref[pick : pick + 1, :], 0.0)
+    before = lax.broadcasted_iota(jnp.int32, (tokens, tokens), 0) < lax.broadcasted_iota(
+        jnp.int32, (tokens, tokens), 1
     )
-    gathered = jnp.dot(
-        placement, returned.reshape(-1, model_width), preferred_element_type=jnp.float32
+    rank = jnp.dot(
+        named.astype(bf16), jnp.where(before, 1.0, 0.0).astype(bf16), preferred_element_type=f32
     )
-    weighted = gathered.reshape(row_count, pick_count, model_width) * route_weights[:, :, None]
-    return jnp.sum(weighted, axis=1)
+    for slot in range(slots):
+        chosen = jnp.where(rank == float(slot), named, 0.0)
+        for side in range(2):
+            part = chosen[side * devices : (side + 1) * devices]
+            place_ref[side, slot] = part.astype(bf16)
+            mix = (part * weight[side * devices : (side + 1) * devices]).T
+            high = mix.astype(bf16)
+            mix_ref[0, side, slot] = high
+            mix_ref[1, side, slot] = (mix - high.astype(f32)).astype(bf16)
+
+    loads[0].wait()
+    squares = jnp.zeros((tokens, 1), f32)
+    for n in range(width // 512):
+        at = pl.ds(n * 512, 512)
+        branch = jnp.dot(head_ref[...], ow_ref[:, at], preferred_element_type=f32)
+        stream = (residual_ref[:, at].astype(f32) + branch).astype(bf16).astype(f32)
+        stream_ref[:, at] = stream
+        squares = squares + jnp.sum(stream * stream, axis=1, keepdims=True)
+    inverse = lax.rsqrt(squares / width + EPSILON)
+    for n in range(width // 512):
+        at = pl.ds(n * 512, 512)
+        x_ref[:, at] = (stream_ref[:, at] * inverse * gain_ref[:, at]).astype(bf16)
+
+    def copy(source, target, send, receive, where):
+        return pltpu.make_async_remote_copy(
+            src_ref=source, dst_ref=target, send_sem=send, recv_sem=receive,
+            device_id=(where // 8, where % 8), device_id_type=MESH,
+        )
+
+    def stage_to(target, side):
+        def one(n, unused):
+            block = stage_ref[pl.ds(n * 384, 384), :].astype(bf16)
+            for k in range(8):
+                target[side, n * 8 + k] = block[k * 48 : (k + 1) * 48]
+            return unused
+
+        lax.fori_loop(0, devices // 8, one, 0)
+
+    def stage_from(source, side):
+        def one(n, unused):
+            for k in range(8):
+                at = n * 384 + k * 48
+                stage_ref[pl.ds(at, 48), :] = source[side, n * 8 + k].astype(f32)
+            return unused
+
+        lax.fori_loop(0, devices // 8, one, 0)
+
+    def exchange(source, target, send, receive, side):
+        def one(n, unused):
+            where = (me + n) % devices
+            copy(source.at[side, where], target.at[side, me], send.at[side], receive.at[side], where).start()
+            return unused
+
+        lax.fori_loop(1, devices, one, 0)
+        pltpu.make_async_copy(source.at[side, me], target.at[side, me], local_sem).start()
+        pltpu.make_async_copy(source.at[side, me], target.at[side, me], local_sem).wait()
+
+    def wait_all(buffer, sem, side):
+        everyone = buffer.at[side, pl.ds(0, devices - 1)]
+        pltpu.make_async_copy(everyone, everyone, sem.at[side]).wait()
+
+    for side in range(2):
+        for slot in range(slots):
+            place = place_ref[side, slot]
+
+            def gather(n, unused):
+                at = pl.multiple_of(n * 512, 512)
+                rows = jnp.dot(place, x_ref[:, pl.ds(at, 512)], preferred_element_type=f32)
+                for k in range(4):
+                    stage_ref[pl.ds(slot * chunks + n * 4 + k, devices, stride=slots * chunks), :] = (
+                        rows[:, k * 128 : (k + 1) * 128]
+                    )
+                return unused
+
+            lax.fori_loop(0, width // 512, gather, 0)
+        stage_to(outgoing, side)
+        exchange(outgoing, arrived, out_send, out_recv, side)
+
+    for one in loads[1:4]:
+        one.wait()
+    gate = jnp.dot(x_ref[...], sg_ref[...], preferred_element_type=f32)
+    up = jnp.dot(x_ref[...], su_ref[...], preferred_element_type=f32)
+    shared = (gate / (1.0 + jnp.exp(-gate)) * up).astype(bf16)
+    for n in range(width // 512):
+        at = pl.ds(n * 512, 512)
+        total_ref[:, at] = stream_ref[:, at] + jnp.dot(
+            shared, sd_ref[:, at], preferred_element_type=f32
+        )
+    for one in loads[4:]:
+        one.wait()
+
+    count = devices * slots
+    for side in range(2):
+        wait_all(arrived, out_recv, side)
+        stage_from(arrived, side)
+        for k in range(chunks):
+            rows_ref[:, pl.ds(k * 128, 128)] = stage_ref[pl.ds(k, count, stride=chunks), :].astype(bf16)
+
+        def inner(n, unused):
+            at = pl.ds(pl.multiple_of(n * 256, 256), 256)
+            gate = jnp.dot(rows_ref[...], eg_ref[side, :, at], preferred_element_type=f32)
+            up = jnp.dot(rows_ref[...], eu_ref[side, :, at], preferred_element_type=f32)
+            hidden_ref[:, at] = (gate / (1.0 + jnp.exp(-gate)) * up).astype(bf16)
+            return unused
+
+        lax.fori_loop(0, hidden // 256, inner, 0)
+
+        def outer(n, unused):
+            at = pl.ds(pl.multiple_of(n * 256, 256), 256)
+            rows = jnp.dot(hidden_ref[...], ed_ref[side, :, at], preferred_element_type=f32)
+            for k in range(2):
+                stage_ref[pl.ds(n * 2 + k, count, stride=chunks), :] = rows[:, k * 128 : (k + 1) * 128]
+            return unused
+
+        lax.fori_loop(0, width // 256, outer, 0)
+        stage_to(result, side)
+        exchange(result, returned, back_send, back_recv, side)
+
+    for side in range(2):
+        wait_all(returned, back_recv, side)
+        stage_from(returned, side)
+        for k in range(chunks):
+            at = pl.ds(k * 128, 128)
+            total = total_ref[:, at]
+            for slot in range(slots):
+                rows = stage_ref[pl.ds(slot * chunks + k, devices, stride=slots * chunks), :].astype(bf16)
+                for level in range(2):
+                    total = total + jnp.dot(
+                        mix_ref[level, side, slot], rows, preferred_element_type=f32
+                    )
+            total_ref[:, at] = total
+    final_ref[...] = total_ref[...].astype(bf16)
+    for side in range(2):
+        wait_all(outgoing, out_send, side)
+        wait_all(result, back_send, side)
+
+
+def mixture(
+    heads, residual, out_weight, norm_gain, shared_gate, shared_up, shared_down,
+    expert_gate, expert_up, expert_down, routed_experts, route_weights,
+):
+    tokens, width = residual.shape
+    hidden = shared_gate.shape[1]
+    bf16, f32 = jnp.bfloat16, jnp.float32
+    vmem, anywhere = pl.BlockSpec(memory_space=pltpu.VMEM), pl.BlockSpec(memory_space=pl.ANY)
+    blocks = (2, 128, 48, 128)
+    return pl.pallas_call(
+        mixture_kernel,
+        out_shape=jax.ShapeDtypeStruct((tokens, width), bf16),
+        in_specs=[vmem] * 5 + [anywhere] * 7,
+        out_specs=vmem,
+        scratch_shapes=[
+            pltpu.VMEM(out_weight.shape, bf16),
+            pltpu.VMEM(shared_gate.shape, bf16),
+            pltpu.VMEM(shared_up.shape, bf16),
+            pltpu.VMEM(shared_down.shape, bf16),
+            pltpu.VMEM(expert_gate.shape, bf16),
+            pltpu.VMEM(expert_up.shape, bf16),
+            pltpu.VMEM(expert_down.shape, bf16),
+            pltpu.VMEM((tokens, width), f32),
+            pltpu.VMEM((tokens, width), bf16),
+            pltpu.VMEM((2, 3, 128, tokens), bf16),
+            pltpu.VMEM((2, 2, 3, tokens, 128), bf16),
+            pltpu.VMEM((128 * 48, 128), f32),
+            pltpu.VMEM(blocks, bf16),
+            pltpu.VMEM(blocks, bf16),
+            pltpu.VMEM((384, width), bf16),
+            pltpu.VMEM((384, hidden), bf16),
+            pltpu.VMEM(blocks, bf16),
+            pltpu.VMEM(blocks, bf16),
+            pltpu.VMEM((tokens, width), f32),
+            pltpu.SemaphoreType.DMA((7,)),
+            pltpu.SemaphoreType.DMA((2,)),
+            pltpu.SemaphoreType.DMA((2,)),
+            pltpu.SemaphoreType.DMA((2,)),
+            pltpu.SemaphoreType.DMA((2,)),
+            pltpu.SemaphoreType.DMA,
+        ],
+        compiler_params=pltpu.CompilerParams(vmem_limit_bytes=60 << 20, has_side_effects=True),
+        name="mixture",
+    )(
+        heads, residual, norm_gain.reshape(1, width), routed_experts.T, route_weights.T,
+        out_weight, shared_gate, shared_up, shared_down, expert_gate, expert_up, expert_down,
+    )
 
 
 def body(
@@ -338,21 +562,21 @@
     routed_experts,
     route_weights,
 ):
-    token_heads = attention(queries, key_heads, value_heads, head_gain)
-    branch = jnp.dot(token_heads, out_weight, preferred_element_type=jnp.float32)
-    stream = (residual.astype(jnp.float32) + branch).astype(jnp.bfloat16)
-    stream_wide = stream.astype(jnp.float32)
-    inverse = lax.rsqrt(jnp.mean(stream_wide * stream_wide, axis=1, keepdims=True) + EPSILON)
-    expert_input = (stream_wide * inverse * norm_gain).astype(jnp.bfloat16)
-    shared_hidden = (
-        jax.nn.silu(jnp.dot(expert_input, shared_gate, preferred_element_type=jnp.float32))
-        * jnp.dot(expert_input, shared_up, preferred_element_type=jnp.float32)
-    ).astype(jnp.bfloat16)
-    shared_term = jnp.dot(shared_hidden, shared_down, preferred_element_type=jnp.float32)
-    routed = routed_sum(
-        expert_input, expert_gate, expert_up, expert_down, routed_experts, route_weights
+    heads = attention(queries, key_heads, value_heads, head_gain)
+    return mixture(
+        heads,
+        residual,
+        out_weight,
+        norm_gain,
+        shared_gate,
+        shared_up,
+        shared_down,
+        expert_gate,
+        expert_up,
+        expert_down,
+        routed_experts,
+        route_weights,
     )
-    return (stream_wide + shared_term + routed).astype(jnp.bfloat16)
 
 
 def solution(mesh):

time: 255 us -> 184 us (0.72)
  Pallas kernels: 84.9 us -> 175 us
  blocking collectives: 51.1 us -> 0 us
  waiting for transfers between devices: 39.4 us -> 0 us
  local copies, waits for them, and re-layouts: 43.1 us -> 6.41 us
  matrix products: 29.1 us -> 0 us
  starting transfers between devices: 5.38 us -> 0 us
    pallas_call x0 -> x1, Pallas kernels: none -> 106 us  [mixture(): pl.pallas_call(mixture_kernel, out_shape=jax.ShapeDtypeStruct((tokens, wi...]
    all_to_all x1 -> x0, blocking collectives: 51.1 us -> none  [routed_sum(): lax.all_to_all(outgoing, ('sp', 'tp'), split_axis=1, concat_axis=1, tiled...]
    all_to_all x1 -> x0, waiting for transfers between devices: 39.4 us -> none  [routed_sum(): lax.all_to_all(result.reshape(arrived.shape), ('sp', 'tp'), split_axis=1,...]
    dot_general x7 -> x0, matrix products: 29.1 us -> none  [the longest x1 10.3 us: routed_sum(): jnp.einsum('erf,efd->erd', hidden, expert_down, preferred_element_type=jn...]
    reshape x3 -> x0, local copies, waits for them, and re-layouts: 26.4 us -> none  [the longest x2 17.6 us: routed_sum(): outgoing.reshape(local_experts, device_count, capacity, model_width)]
    pallas_call x1, Pallas kernels: 84.9 us -> 68.6 us  [attention(): pl.pallas_call(attention_kernel, out_shape=jax.ShapeDtypeStruct((128, 8 *...]
    convert_element_type x1 -> x0, local copies, waits for them, and re-layouts: 6.85 us -> none  [routed_sum(): result = jnp.einsum('erf,efd->erd', hidden, expert_down, preferred_elemen...]
    all_to_all x1 -> x0, local copies, waits for them, and re-layouts: 6.03 us -> none  [routed_sum(): lax.all_to_all(result.reshape(arrived.shape), ('sp', 'tp'), split_axis=1,...]
  transfers between devices with their start and end apart: 1 -> 0, of which waited for: 1 -> 0; matrix products, arithmetic and copies ran while one was open for 1% -> 0% of each run, Pallas kernels for 0% -> 0%
where the time goes in v3:
time: 184 us; the launch traced here: 181 us
  Pallas kernels  175 us (95%)
  local copies, waits for them, and re-layouts  6.41 us (3%)
    pallas_call x1, Pallas kernels, mixture(): pl.pallas_call(mixture_kernel, out_shape=jax.ShapeDtypeStruct((tokens, wi...  106 us
    pallas_call x1, Pallas kernels, attention(): pl.pallas_call(attention_kernel, out_shape=jax.ShapeDtypeStruct((128, 8 *...  68.6 us
    unnamed x8, local copies, waits for them, and re-layouts  6.41 us

profile of v3, /device:TPU:1, one launch (start us, length us, event | category | flops | bytes accessed | tf_op | source)
XLA Modules:
  0.0 181.0 jit_solution(11415713257857782815)
XLA Ops:
  0.0 1.1 copy.16.q_ref
  1.1 1.1 copy.17.k_ref
  2.2 1.1 copy.18.v_ref
  3.2 0.0 copy-start.1
  3.3 0.6 copy-done.1
  3.9 68.6 %attention.1.head_ref = bf16[128,512]{1,0:T(8,128)(2,1)S(1)} custom-call(bf16[1024,64]{1,0:T(8,128)(2,1)S(1)} %copy.16.q_ref, bf16[1024,64]{1,0:T(8,128)(2,1)S(1)} %copy.17.k_ref, bf16[1024,64]{1,0:T(8,128)(2,1)S(1)} %copy.18.v_ref, f32[1,64]{1,0:T(1,128)S(1)} %bitcast.4), custom_call_target="tpu_custom_call" | custom-call | tf_op jit(solution)/shard_map/attention/pallas_call | solution.py:288
  72.5 0.0 copy-start
  72.5 0.6 copy-done
  73.2 106.0 %mixture.1 = bf16[128,2048]{1,0:T(8,128)(2,1)} custom-call(bf16[128,512]{1,0:T(8,128)(2,1)} %copy-done, bf16[128,2048]{1,0:T(8,128)(2,1)} %residual_ref.1, f32[1,2048]{1,0:T(1,128)} %bitcast.5, s32[4,128]{1,0:T(4,128)} %bitcast.6, f32[4,128]{1,0:T(4,128)} %bitcast.7, bf16[512,2048]{1,0:T(8,128)(2,1)} %out_weight.1, bf16[2048,512]{1,0:T(8,128)(2,1)} %shared_gate.1, ...), custom_call_target="tpu_custom_call" | custom-call | tf_op jit(solution)/shard_map/mixture/pallas_call | solution.py:508
  179.2 1.9 %copy.20 = bf16[128,2048]{1,0:T(8,128)(2,1)} copy(bf16[128,2048]{1,0:T(8,128)(2,1)} %mixture.1) | data formatting | bytes 1048576
Async XLA Ops:
  3.2 0.7 copy-start.1
  72.5 0.7 copy-start

commit v4 on v3

--- a/solution.py
+++ b/solution.py
@@ -20,7 +20,8 @@
 
 def tile_terms(q2, keys, values, tri, carry, mask):
     x = jnp.dot(q2, keys, preferred_element_type=jnp.float32)
-    drop = jnp.maximum(jnp.log(1.0 + jnp.exp2(jnp.minimum(x, 126.0))) * LOG2E, x)
+    x = jnp.minimum(x, 126.0)
+    drop = jnp.log(1.0 + jnp.exp2(x)) * LOG2E
     stick = x - drop
     if mask is not None:
         drop = jnp.where(mask, drop, 0.0)
@@ -37,7 +38,7 @@
 def attention_kernel(
     q_ref, k_ref, v_ref, gain_ref, out_ref,
     q_own, q_ref2, key_ref, value_ref, acc_ref, carry_ref, sum_ref, past_ref, tri_ref, out_own, out_in,
-    q_send, q_recv, q_local, send_sem, key_recv, value_recv, out_send, out_recv, out_local,
+    q_send, q_recv, send_sem, key_recv, value_recv, out_send, out_recv, out_local,
 ):
     me, head = lax.axis_index("sp"), lax.axis_index("tp")
     row, column = me // 4, me % 4
@@ -47,8 +48,8 @@
     high = q.astype(jnp.bfloat16)
     low = (q - high.astype(jnp.float32)).astype(jnp.bfloat16)
     both = jnp.concatenate([high, low], axis=1)
-    q_own[0] = both[:half]
-    q_own[1] = both[half:]
+    q_ref2[0] = both[:half]
+    q_own[...] = both[half:]
     for part in range(8):
         block = k_ref[pl.ds(part * 128, 128), :].astype(jnp.float32)
         key_ref[me, pl.ds(part * HEAD_DIM, HEAD_DIM), :] = block.T.astype(jnp.bfloat16)
@@ -61,19 +62,8 @@
             device_id=(where, which), device_id_type=MESH,
         )
 
-    slot = jnp.where(me < 8, 1, 0)
-    for part in range(2):
-        place = 2 * me + part
-        owner = jnp.where(place < 16, place, 31 - place)
-
-        @pl.when(owner != me)
-        def _():
-            copy(q_own.at[part], q_ref2.at[slot], q_send.at[part], q_recv.at[slot], owner, head).start()
-
-        @pl.when(owner == me)
-        def _():
-            pltpu.make_async_copy(q_own.at[part], q_ref2.at[slot], q_local).start()
-
+    q_copy = copy(q_own, q_ref2.at[1], q_send, q_recv, 15 - me, head)
+    q_copy.start()
     steps = (1, 3, 2)
 
     def key_copy(block, n, where):
@@ -133,16 +123,18 @@
             values = value_ref[block, pl.ds(part * TILE, TILE), :]
             lanes = lax.broadcasted_iota(jnp.int32, values.shape, 1) // HEAD_DIM
             values = jnp.where(lanes == side, values, jnp.zeros_like(values))
-            for tile in range(2):
-                if diagonal and tile < part:
-                    continue
-                rows = pl.ds(tile * TILE, TILE)
-                mask = c < r if diagonal and tile == part else None
-                out, carry = tile_terms(
-                    q_ref2[which, rows, :], keys, values, tri_ref[...], carry_ref[which, block, rows, :], mask
+            rows, mask = pl.ds(0, half), None
+            if diagonal and part == 1:
+                rows, mask = pl.ds(TILE, TILE), c < r
+            elif diagonal:
+                mask = lax.broadcasted_iota(jnp.int32, (half, TILE), 1) < lax.broadcasted_iota(
+                    jnp.int32, (half, TILE), 0
                 )
-                acc_ref[which, block, rows, :] += out
-                carry_ref[which, block, rows, :] = carry
+            out, carry = tile_terms(
+                q_ref2[which, rows, :], keys, values, tri_ref[...], carry_ref[which, block, rows, :], mask
+            )
+            acc_ref[which, block, rows, :] += out
+            carry_ref[which, block, rows, :] = carry
 
     def finish(which, place):
         blank = jnp.zeros((half, 128), jnp.float32)
@@ -177,19 +169,7 @@
             def _():
                 pltpu.make_async_copy(out_own.at[n], out_in.at[head], out_local).start()
 
-    @pl.when(me != 10)
-    def _():
-        copy(q_own.at[0], q_ref2.at[0], q_send.at[0], q_recv.at[0], me, head).wait_recv()
-
-    @pl.when(me != 0)
-    def _():
-        copy(q_own.at[0], q_ref2.at[1], q_send.at[0], q_recv.at[1], me, head).wait_recv()
-
-    @pl.when((me == 0) | (me == 10))
-    def _():
-        pltpu.make_async_copy(q_own.at[0], q_ref2.at[0], q_local).wait()
-
-    far = 31 - me
+    far = jnp.maximum(2 * me, 31 - 2 * me)
     order = ((0, 0), (0, 1), (1, 0), (0, 3), (3, 0), (0, 2), (2, 0), (1, 1), (3, 3), (1, 3), (3, 1), (1, 2), (2, 1), (3, 2), (2, 3), (2, 2))
 
     def pick(n, axis):
@@ -208,8 +188,12 @@
 
         def pair(i, unused):
             which, side = i // 2, 1 - i % 2
-            top = jnp.where(which == 0, far, me)
+            top = jnp.where(which == 0, 2 * me, 31 - 2 * me)
             place = 2 * block + side
+
+            @pl.when((n == 0) & (i == 2))
+            def _():
+                q_copy.wait_recv()
 
             @pl.when((side == 1) & (2 * block <= top))
             def _():
@@ -233,8 +217,8 @@
         return unused
 
     lax.fori_loop(0, 16, visit, 0)
-    finish(0, far)
-    finish(1, me)
+    finish(0, 2 * me)
+    finish(1, 31 - 2 * me)
 
     def drain(n, unused):
         @pl.when(n != me)
@@ -244,23 +228,15 @@
         return unused
 
     lax.fori_loop(far // 2 + 1, 16, drain, 0)
-    for part in range(2):
-        place = 2 * me + part
-        owner = jnp.where(place < 16, place, 31 - place)
-
-        @pl.when(owner != me)
-        def _():
-            copy(q_own.at[part], q_ref2.at[slot], q_send.at[part], q_recv.at[slot], owner, head).wait_send()
+    q_copy.wait_send()
     for one in sent + passed:
         one.wait_send()
 
-    place = 2 * me + head // 4
-    owner = jnp.where(place < 16, place, 31 - place)
     for other in range(8):
-        @pl.when(jnp.logical_not((owner == me) & (other == head)))
+        @pl.when(jnp.logical_not((head < 4) & (other == head)))
         def _():
             copy(out_own.at[0], out_in.at[other], out_send.at[0], out_recv.at[other], me, head).wait_recv()
-    for which, spot in ((0, far), (1, me)):
+    for which, spot in ((0, 2 * me), (1, 31 - 2 * me)):
         for piece in range(4):
             n = 4 * which + piece
             where, token = spot // 2, (spot % 2) * 4 + piece
@@ -291,7 +267,7 @@
         in_specs=[pl.BlockSpec(memory_space=pltpu.VMEM)] * 4,
         out_specs=pl.BlockSpec(memory_space=pltpu.VMEM),
         scratch_shapes=[
-            pltpu.VMEM((2, half, 128), jnp.bfloat16),
+            pltpu.VMEM((half, 128), jnp.bfloat16),
             pltpu.VMEM((2, half, 128), jnp.bfloat16),
             pltpu.VMEM((16, half, 128), jnp.bfloat16),
             pltpu.VMEM((16, half, 128), jnp.bfloat16),
@@ -302,8 +278,7 @@
             pltpu.VMEM((TILE, TILE), jnp.bfloat16),
             pltpu.VMEM((8, 64, 128), jnp.bfloat16),
             pltpu.VMEM((8, 64, 128), jnp.bfloat16),
-            pltpu.SemaphoreType.DMA((2,)),
-            pltpu.SemaphoreType.DMA((2,)),
+            pltpu.SemaphoreType.DMA,
             pltpu.SemaphoreType.DMA,
             pltpu.SemaphoreType.DMA((30,)),
             pltpu.SemaphoreType.DMA((16,)),
@@ -408,7 +383,7 @@
 
     def exchange(source, target, send, receive, side):
         def one(n, unused):
-            where = (me + n) % devices
+            where = (me + 37 * n) % devices
             copy(source.at[side, where], target.at[side, me], send.at[side], receive.at[side], where).start()
             return unused
 

time: 184 us -> 168 us (0.913); the launches traced: 181 us -> 168 us
  Pallas kernels: 175 us -> 162 us
    pallas_call x1, Pallas kernels: 106 us -> 97.6 us  [mixture(): pl.pallas_call(mixture_kernel, out_shape=jax.ShapeDtypeStruct((tokens, wi...]
    pallas_call x1, Pallas kernels: 68.6 us -> 63.9 us  [attention(): pl.pallas_call(attention_kernel, out_shape=jax.ShapeDtypeStruct((128, 8 *...]
where the time goes in v4:
time: 168 us
  Pallas kernels  162 us (96%)
  local copies, waits for them, and re-layouts  6.41 us (4%)
    pallas_call x1, Pallas kernels, mixture(): pl.pallas_call(mixture_kernel, out_shape=jax.ShapeDtypeStruct((tokens, wi...  97.6 us
    pallas_call x1, Pallas kernels, attention(): pl.pallas_call(attention_kernel, out_shape=jax.ShapeDtypeStruct((128, 8 *...  63.9 us
    unnamed x8, local copies, waits for them, and re-layouts  6.41 us

profile of v4, /device:TPU:1, one launch (start us, length us, event | category | flops | bytes accessed | tf_op | source)
XLA Modules:
  0.0 168.0 jit_solution(4241772696222772540)
XLA Ops:
  0.0 1.1 copy.16.q_ref
  1.1 1.1 copy.17.k_ref
  2.2 1.1 copy.18.v_ref
  3.2 0.0 copy-start.1
  3.3 0.6 copy-done.1
  3.9 63.9 %attention.1.head_ref = bf16[128,512]{1,0:T(8,128)(2,1)S(1)} custom-call(bf16[1024,64]{1,0:T(8,128)(2,1)S(1)} %copy.16.q_ref, bf16[1024,64]{1,0:T(8,128)(2,1)S(1)} %copy.17.k_ref, bf16[1024,64]{1,0:T(8,128)(2,1)S(1)} %copy.18.v_ref, f32[1,64]{1,0:T(1,128)S(1)} %bitcast.4), custom_call_target="tpu_custom_call" | custom-call | tf_op jit(solution)/shard_map/attention/pallas_call | solution.py:264
  67.9 0.0 copy-start
  67.9 0.6 copy-done
  68.5 97.6 %mixture.1 = bf16[128,2048]{1,0:T(8,128)(2,1)} custom-call(bf16[128,512]{1,0:T(8,128)(2,1)} %copy-done, bf16[128,2048]{1,0:T(8,128)(2,1)} %residual_ref.1, f32[1,2048]{1,0:T(1,128)} %bitcast.5, s32[4,128]{1,0:T(4,128)} %bitcast.6, f32[4,128]{1,0:T(4,128)} %bitcast.7, bf16[512,2048]{1,0:T(8,128)(2,1)} %out_weight.1, bf16[2048,512]{1,0:T(8,128)(2,1)} %shared_gate.1, ...), custom_call_target="tpu_custom_call" | custom-call | tf_op jit(solution)/shard_map/mixture/pallas_call | solution.py:483
  166.1 1.9 %copy.20 = bf16[128,2048]{1,0:T(8,128)(2,1)} copy(bf16[128,2048]{1,0:T(8,128)(2,1)} %mixture.1) | data formatting | bytes 1048576
Async XLA Ops:
  3.2 0.7 copy-start.1
  67.9 0.7 copy-start

commit v5 on v4

--- a/solution.py
+++ b/solution.py
@@ -35,25 +35,112 @@
     return out, carry + jnp.broadcast_to(total, carry.shape)
 
 
+def remote(source, target, send, receive, where):
+    return pltpu.make_async_remote_copy(
+        src_ref=source, dst_ref=target, send_sem=send, recv_sem=receive,
+        device_id=where, device_id_type=MESH,
+    )
+
+
+def route(expert_ref, route_ref, place_ref, mix_ref):
+    devices, slots, tokens = 128, 3, expert_ref.shape[1]
+    f32, bf16 = jnp.float32, jnp.bfloat16
+    line = lax.broadcasted_iota(jnp.int32, (2 * devices, tokens), 0)
+    expert = 2 * (line % devices) + line // devices
+    named = jnp.zeros((2 * devices, tokens), f32)
+    weight = jnp.zeros((2 * devices, tokens), f32)
+    for pick in range(expert_ref.shape[0]):
+        hit = expert_ref[pick : pick + 1, :] == expert
+        named = named + jnp.where(hit, 1.0, 0.0)
+        if mix_ref is not None:
+            weight = weight + jnp.where(hit, route_ref[pick : pick + 1, :], 0.0)
+    before = lax.broadcasted_iota(jnp.int32, (tokens, tokens), 0) < lax.broadcasted_iota(
+        jnp.int32, (tokens, tokens), 1
+    )
+    rank = jnp.dot(
+        named.astype(bf16), jnp.where(before, 1.0, 0.0).astype(bf16), preferred_element_type=f32
+    )
+    for slot in range(slots):
+        chosen = jnp.where(rank == float(slot), named, 0.0)
+        for side in range(2):
+            part = chosen[side * devices : (side + 1) * devices]
+            place_ref[side, slot] = part.astype(bf16)
+            if mix_ref is not None:
+                mix = (part * weight[side * devices : (side + 1) * devices]).T
+                high = mix.astype(bf16)
+                mix_ref[0, side, slot] = high
+                mix_ref[1, side, slot] = (mix - high.astype(f32)).astype(bf16)
+
+
+def collect(place_ref, side, from_ref, stage_ref, outgoing):
+    for slot in range(3):
+        place = place_ref[side, slot]
+
+        def gather(n, unused):
+            at = pl.multiple_of(n * 512, 512)
+            rows = jnp.dot(place, from_ref[:, pl.ds(at, 512)], preferred_element_type=jnp.float32)
+            for k in range(4):
+                stage_ref[pl.ds(slot * 16 + n * 4 + k, 128, stride=48), :] = (
+                    rows[:, k * 128 : (k + 1) * 128]
+                )
+            return unused
+
+        lax.fori_loop(0, from_ref.shape[1] // 512, gather, 0)
+
+    def move(n, unused):
+        block = stage_ref[pl.ds(n * 384, 384), :].astype(jnp.bfloat16)
+        for k in range(8):
+            outgoing[n * 8 + k] = block[k * 48 : (k + 1) * 48]
+        return unused
+
+    lax.fori_loop(0, 16, move, 0)
+
+
+def spread(source, target, send, receive, own, me):
+    def go(n):
+        where = lax.rem(me + 37 * n, 128)
+        device = (lax.div(where, 8), lax.rem(where, 8))
+        remote(source.at[where], target.at[me], send, receive, device).start()
+
+    def several(n, unused):
+        for k in range(7):
+            go(7 * n + k + 1)
+        return unused
+
+    lax.fori_loop(0, 18, several, 0)
+    go(127)
+    pltpu.make_async_copy(source.at[me], target.at[me], own).start()
+
+
+def spread_own(source, target, own, me):
+    pltpu.make_async_copy(source.at[me], target.at[me], own).wait()
+
+
+def spread_wait(buffer, sem):
+    everyone = buffer.at[pl.ds(0, 127)]
+    pltpu.make_async_copy(everyone, everyone, sem).wait()
+
+
 def attention_kernel(
-    q_ref, k_ref, v_ref, gain_ref, out_ref,
+    q_ref, k_ref, v_ref, gain_ref, residual_ref, expert_ref, out_ref, arrived_ref,
     q_own, q_ref2, key_ref, value_ref, acc_ref, carry_ref, sum_ref, past_ref, tri_ref, out_own, out_in,
+    place_ref, stage_ref, outgoing,
     q_send, q_recv, send_sem, key_recv, value_recv, out_send, out_recv, out_local,
+    row_send, row_recv, row_local,
 ):
     me, head = lax.axis_index("sp"), lax.axis_index("tp")
     row, column = me // 4, me % 4
-    half = q_ref.shape[0] // 2
-
-    q = q_ref[...].astype(jnp.float32) * (LOG2E / math.sqrt(HEAD_DIM))
+    half = q_ref.shape[1] // 2
+
+    q = q_ref[...].astype(jnp.float32).T * (LOG2E / math.sqrt(HEAD_DIM))
     high = q.astype(jnp.bfloat16)
     low = (q - high.astype(jnp.float32)).astype(jnp.bfloat16)
     both = jnp.concatenate([high, low], axis=1)
     q_ref2[0] = both[:half]
     q_own[...] = both[half:]
     for part in range(8):
-        block = k_ref[pl.ds(part * 128, 128), :].astype(jnp.float32)
-        key_ref[me, pl.ds(part * HEAD_DIM, HEAD_DIM), :] = block.T.astype(jnp.bfloat16)
-    v = v_ref[...].astype(jnp.float32)
+        key_ref[me, pl.ds(part * HEAD_DIM, HEAD_DIM), :] = k_ref[:, pl.ds(part * 128, 128)]
+    v = v_ref[...].astype(jnp.float32).T
     value_ref[me] = jnp.concatenate([v[:half], v[half:]], axis=1).astype(jnp.bfloat16)
 
     def copy(source, target, out_sem, in_sem, where, which):
@@ -87,6 +174,9 @@
     r = lax.broadcasted_iota(jnp.int32, (TILE, TILE), 0)
     c = lax.broadcasted_iota(jnp.int32, (TILE, TILE), 1)
     tri_ref[...] = (r > c).astype(jnp.float32).astype(jnp.bfloat16)
+    route(expert_ref, None, place_ref, None)
+    collect(place_ref, 0, residual_ref, stage_ref, outgoing)
+
     passed = []
 
     def forward():
@@ -182,6 +272,10 @@
         def _():
             forward()
 
+        @pl.when(n == 10)
+        def _():
+            spread(outgoing, arrived_ref, row_send, row_recv, row_local, me * 8 + head)
+
         @pl.when((block <= far // 2) & (n > 0))
         def _():
             arrived(block)
@@ -256,16 +350,22 @@
         one = jnp.concatenate([one[:, :HEAD_DIM], one[:, HEAD_DIM:]], axis=0)
         two = jnp.concatenate([two[:, :HEAD_DIM], two[:, HEAD_DIM:]], axis=0)
         out_ref[:, pl.ds(pair * 128, 128)] = jnp.concatenate([one, two], axis=1).astype(jnp.bfloat16)
-
-
-def attention(queries, key_heads, value_heads, head_gain):
+    spread_own(outgoing, arrived_ref, row_local, me * 8 + head)
+    spread_wait(arrived_ref, row_recv)
+    spread_wait(outgoing, row_send)
+
+
+def attention(queries, key_heads, value_heads, head_gain, residual, routed_experts):
     rows = queries.shape[0]
     half = rows // 2
     return pl.pallas_call(
         attention_kernel,
-        out_shape=jax.ShapeDtypeStruct((128, 8 * HEAD_DIM), jnp.bfloat16),
-        in_specs=[pl.BlockSpec(memory_space=pltpu.VMEM)] * 4,
-        out_specs=pl.BlockSpec(memory_space=pltpu.VMEM),
+        out_shape=(
+            jax.ShapeDtypeStruct((128, 8 * HEAD_DIM), jnp.bfloat16),
+            jax.ShapeDtypeStruct((128, 48, 128), jnp.bfloat16),
+        ),
+        in_specs=[pl.BlockSpec(memory_space=pltpu.VMEM)] * 6,
+        out_specs=[pl.BlockSpec(memory_space=pltpu.VMEM)] * 2,
         scratch_shapes=[
             pltpu.VMEM((half, 128), jnp.bfloat16),
             pltpu.VMEM((2, half, 128), jnp.bfloat16),
@@ -278,6 +378,9 @@
             pltpu.VMEM((TILE, TILE), jnp.bfloat16),
             pltpu.VMEM((8, 64, 128), jnp.bfloat16),
             pltpu.VMEM((8, 64, 128), jnp.bfloat16),
+            pltpu.VMEM((2, 3, 128, 128), jnp.bfloat16),
+            pltpu.VMEM((128 * 48, 128), jnp.float32),
+            pltpu.VMEM((128, 48, 128), jnp.bfloat16),
             pltpu.SemaphoreType.DMA,
             pltpu.SemaphoreType.DMA,
             pltpu.SemaphoreType.DMA((30,)),
@@ -286,20 +389,24 @@
             pltpu.SemaphoreType.DMA((8,)),
             pltpu.SemaphoreType.DMA((8,)),
             pltpu.SemaphoreType.DMA,
+            pltpu.SemaphoreType.DMA,
+            pltpu.SemaphoreType.DMA,
+            pltpu.SemaphoreType.DMA,
         ],
-        compiler_params=pltpu.CompilerParams(vmem_limit_bytes=40 << 20, has_side_effects=True),
+        compiler_params=pltpu.CompilerParams(vmem_limit_bytes=56 << 20, has_side_effects=True),
         name="attention",
-    )(queries, key_heads, value_heads, head_gain.reshape(1, HEAD_DIM))
+    )(queries.T, key_heads.T, value_heads.T, head_gain.reshape(1, HEAD_DIM), residual, routed_experts)
 
 
 def mixture_kernel(
-    head_ref, residual_ref, gain_ref, expert_ref, route_ref,
+    head_ref, arrived, residual_ref, gain_ref, expert_ref, route_ref,
     out_weight, shared_gate, shared_up, shared_down, expert_gate, expert_up, expert_down,
     final_ref,
     ow_ref, sg_ref, su_ref, sd_ref, eg_ref, eu_ref, ed_ref,
-    stream_ref, x_ref, place_ref, mix_ref, stage_ref, outgoing, arrived, rows_ref, hidden_ref,
+    stream_ref, x_ref, place_ref, mix_ref, stage_ref, head_stage, head_out, head_in, head_rows,
+    rows_ref, hidden_ref, outgoing, incoming,
     result, returned, total_ref,
-    load_sem, out_send, out_recv, back_send, back_recv, local_sem,
+    load_sem, head_send, head_recv, head_local, row_send, row_recv, row_local, back_send, back_recv, local_sem,
 ):
     me = lax.axis_index("sp") * 8 + lax.axis_index("tp")
     tokens, width = residual_ref.shape
@@ -320,29 +427,21 @@
     for one in loads:
         one.start()
 
-    line = lax.broadcasted_iota(jnp.int32, (2 * devices, tokens), 0)
-    expert = 2 * (line % devices) + line // devices
-    named = jnp.zeros((2 * devices, tokens), f32)
-    weight = jnp.zeros((2 * devices, tokens), f32)
-    for pick in range(expert_ref.shape[0]):
-        hit = expert_ref[pick : pick + 1, :] == expert
-        named = named + jnp.where(hit, 1.0, 0.0)
-        weight = weight + jnp.where(hit, route_ref[pick : pick + 1, :], 0.0)
-    before = lax.broadcasted_iota(jnp.int32, (tokens, tokens), 0) < lax.broadcasted_iota(
-        jnp.int32, (tokens, tokens), 1
-    )
-    rank = jnp.dot(
-        named.astype(bf16), jnp.where(before, 1.0, 0.0).astype(bf16), preferred_element_type=f32
-    )
+    route(expert_ref, route_ref, place_ref, mix_ref)
+    head_stage[...] = jnp.zeros_like(head_stage)
     for slot in range(slots):
-        chosen = jnp.where(rank == float(slot), named, 0.0)
-        for side in range(2):
-            part = chosen[side * devices : (side + 1) * devices]
-            place_ref[side, slot] = part.astype(bf16)
-            mix = (part * weight[side * devices : (side + 1) * devices]).T
-            high = mix.astype(bf16)
-            mix_ref[0, side, slot] = high
-            mix_ref[1, side, slot] = (mix - high.astype(f32)).astype(bf16)
+        rows = jnp.dot(place_ref[0, slot], head_ref[...], preferred_element_type=f32)
+        for k in range(4):
+            head_stage[pl.ds(slot * 4 + k, devices, stride=16), :] = rows[:, k * 128 : (k + 1) * 128]
+
+    def pack(n, unused):
+        block = head_stage[pl.ds(n * 128, 128), :].astype(bf16)
+        for k in range(8):
+            head_out[n * 8 + k] = block[k * 16 : (k + 1) * 16]
+        return unused
+
+    lax.fori_loop(0, devices // 8, pack, 0)
+    spread(head_out, head_in, head_send, head_recv, head_local, me)
 
     loads[0].wait()
     squares = jnp.zeros((tokens, 1), f32)
@@ -357,11 +456,8 @@
         at = pl.ds(n * 512, 512)
         x_ref[:, at] = (stream_ref[:, at] * inverse * gain_ref[:, at]).astype(bf16)
 
-    def copy(source, target, send, receive, where):
-        return pltpu.make_async_remote_copy(
-            src_ref=source, dst_ref=target, send_sem=send, recv_sem=receive,
-            device_id=(where // 8, where % 8), device_id_type=MESH,
-        )
+    collect(place_ref, 1, x_ref, stage_ref, outgoing)
+    spread(outgoing, incoming, row_send, row_recv, row_local, me)
 
     def stage_to(target, side):
         def one(n, unused):
@@ -372,45 +468,22 @@
 
         lax.fori_loop(0, devices // 8, one, 0)
 
-    def stage_from(source, side):
+    def stage_from(source):
         def one(n, unused):
             for k in range(8):
                 at = n * 384 + k * 48
-                stage_ref[pl.ds(at, 48), :] = source[side, n * 8 + k].astype(f32)
+                stage_ref[pl.ds(at, 48), :] = source(n * 8 + k).astype(f32)
             return unused
 
         lax.fori_loop(0, devices // 8, one, 0)
 
     def exchange(source, target, send, receive, side):
-        def one(n, unused):
-            where = (me + 37 * n) % devices
-            copy(source.at[side, where], target.at[side, me], send.at[side], receive.at[side], where).start()
-            return unused
-
-        lax.fori_loop(1, devices, one, 0)
-        pltpu.make_async_copy(source.at[side, me], target.at[side, me], local_sem).start()
-        pltpu.make_async_copy(source.at[side, me], target.at[side, me], local_sem).wait()
+        spread(source.at[side], target.at[side], send.at[side], receive.at[side], local_sem, me)
+        spread_own(source.at[side], target.at[side], local_sem, me)
 
     def wait_all(buffer, sem, side):
         everyone = buffer.at[side, pl.ds(0, devices - 1)]
         pltpu.make_async_copy(everyone, everyone, sem.at[side]).wait()
-
-    for side in range(2):
-        for slot in range(slots):
-            place = place_ref[side, slot]
-
-            def gather(n, unused):
-                at = pl.multiple_of(n * 512, 512)
-                rows = jnp.dot(place, x_ref[:, pl.ds(at, 512)], preferred_element_type=f32)
-                for k in range(4):
-                    stage_ref[pl.ds(slot * chunks + n * 4 + k, devices, stride=slots * chunks), :] = (
-                        rows[:, k * 128 : (k + 1) * 128]
-                    )
-                return unused
-
-            lax.fori_loop(0, width // 512, gather, 0)
-        stage_to(outgoing, side)
-        exchange(outgoing, arrived, out_send, out_recv, side)
 
     for one in loads[1:4]:
         one.wait()
@@ -425,12 +498,57 @@
     for one in loads[4:]:
         one.wait()
 
-    count = devices * slots
+    spread_own(head_out, head_in, head_local, me)
+    spread_wait(head_in, head_recv)
+
+    def unpack(n, unused):
+        for k in range(8):
+            head_stage[pl.ds(n * 128 + k * 16, 16), :] = head_in[n * 8 + k].astype(f32)
+        return unused
+
+    lax.fori_loop(0, devices // 8, unpack, 0)
+
+    def first_rows():
+        stage_from(lambda at: arrived[at])
+        for slot in range(slots):
+            for k in range(4):
+                head_rows[pl.ds(slot * devices, devices), pl.ds(k * 128, 128)] = head_stage[
+                    pl.ds(slot * 4 + k, devices, stride=16), :
+                ].astype(bf16)
+        for slot in range(slots):
+            rows = pl.ds(slot * devices, devices)
+            squares = jnp.zeros((devices, 1), f32)
+            for n in range(width // 512):
+                at = pl.ds(n * 512, 512)
+                branch = jnp.dot(head_rows[rows, :], ow_ref[:, at], preferred_element_type=f32)
+                base = jnp.concatenate(
+                    [
+                        stage_ref[pl.ds(slot * chunks + n * 4 + k, devices, stride=slots * chunks), :]
+                        for k in range(4)
+                    ],
+                    axis=1,
+                )
+                stream = (base + branch).astype(bf16)
+                rows_ref[rows, at] = stream
+                stream = stream.astype(f32)
+                squares = squares + jnp.sum(stream * stream, axis=1, keepdims=True)
+            inverse = lax.rsqrt(squares / width + EPSILON)
+            for n in range(width // 512):
+                at = pl.ds(n * 512, 512)
+                rows_ref[rows, at] = (rows_ref[rows, at].astype(f32) * inverse * gain_ref[:, at]).astype(bf16)
+
+    def second_rows():
+        spread_own(outgoing, incoming, row_local, me)
+        spread_wait(incoming, row_recv)
+        stage_from(lambda at: incoming[at])
+        for slot in range(slots):
+            for k in range(chunks):
+                rows_ref[pl.ds(slot * devices, devices), pl.ds(k * 128, 128)] = stage_ref[
+                    pl.ds(slot * chunks + k, devices, stride=slots * chunks), :
+                ].astype(bf16)
+
     for side in range(2):
-        wait_all(arrived, out_recv, side)
-        stage_from(arrived, side)
-        for k in range(chunks):
-            rows_ref[:, pl.ds(k * 128, 128)] = stage_ref[pl.ds(k, count, stride=chunks), :].astype(bf16)
+        (first_rows, second_rows)[side]()
 
         def inner(n, unused):
             at = pl.ds(pl.multiple_of(n * 256, 256), 256)
@@ -444,8 +562,11 @@
         def outer(n, unused):
             at = pl.ds(pl.multiple_of(n * 256, 256), 256)
             rows = jnp.dot(hidden_ref[...], ed_ref[side, :, at], preferred_element_type=f32)
-            for k in range(2):
-                stage_ref[pl.ds(n * 2 + k, count, stride=chunks), :] = rows[:, k * 128 : (k + 1) * 128]
+            for slot in range(slots):
+                for k in range(2):
+                    stage_ref[pl.ds(slot * chunks + n * 2 + k, devices, stride=slots * chunks), :] = (
+                        rows[slot * devices : (slot + 1) * devices, k * 128 : (k + 1) * 128]
+                    )
             return unused
 
         lax.fori_loop(0, width // 256, outer, 0)
@@ -454,7 +575,7 @@
 
     for side in range(2):
         wait_all(returned, back_recv, side)
-        stage_from(returned, side)
+        stage_from(lambda at: returned[side, at])
         for k in range(chunks):
             at = pl.ds(k * 128, 128)
             total = total_ref[:, at]
@@ -466,13 +587,14 @@
                     )
             total_ref[:, at] = total
     final_ref[...] = total_ref[...].astype(bf16)
+    spread_wait(head_out, head_send)
+    spread_wait(outgoing, row_send)
     for side in range(2):
-        wait_all(outgoing, out_send, side)
         wait_all(result, back_send, side)
 
 
 def mixture(
-    heads, residual, out_weight, norm_gain, shared_gate, shared_up, shared_down,
+    heads, arrived, residual, out_weight, norm_gain, shared_gate, shared_up, shared_down,
     expert_gate, expert_up, expert_down, routed_experts, route_weights,
 ):
     tokens, width = residual.shape
@@ -483,7 +605,7 @@
     return pl.pallas_call(
         mixture_kernel,
         out_shape=jax.ShapeDtypeStruct((tokens, width), bf16),
-        in_specs=[vmem] * 5 + [anywhere] * 7,
+        in_specs=[vmem] * 6 + [anywhere] * 7,
         out_specs=vmem,
         scratch_shapes=[
             pltpu.VMEM(out_weight.shape, bf16),
@@ -498,16 +620,24 @@
             pltpu.VMEM((2, 3, 128, tokens), bf16),
             pltpu.VMEM((2, 2, 3, tokens, 128), bf16),
             pltpu.VMEM((128 * 48, 128), f32),
-            pltpu.VMEM(blocks, bf16),
-            pltpu.VMEM(blocks, bf16),
+            pltpu.VMEM((128 * 16, 128), f32),
+            pltpu.VMEM((128, 16, 128), bf16),
+            pltpu.VMEM((128, 16, 128), bf16),
+            pltpu.VMEM((384, 512), bf16),
             pltpu.VMEM((384, width), bf16),
             pltpu.VMEM((384, hidden), bf16),
+            pltpu.VMEM((128, 48, 128), bf16),
+            pltpu.VMEM((128, 48, 128), bf16),
             pltpu.VMEM(blocks, bf16),
             pltpu.VMEM(blocks, bf16),
             pltpu.VMEM((tokens, width), f32),
             pltpu.SemaphoreType.DMA((7,)),
-            pltpu.SemaphoreType.DMA((2,)),
-            pltpu.SemaphoreType.DMA((2,)),
+            pltpu.SemaphoreType.DMA,
+            pltpu.SemaphoreType.DMA,
+            pltpu.SemaphoreType.DMA,
+            pltpu.SemaphoreType.DMA,
+            pltpu.SemaphoreType.DMA,
+            pltpu.SemaphoreType.DMA,
             pltpu.SemaphoreType.DMA((2,)),
             pltpu.SemaphoreType.DMA((2,)),
             pltpu.SemaphoreType.DMA,
@@ -515,7 +645,7 @@
         compiler_params=pltpu.CompilerParams(vmem_limit_bytes=60 << 20, has_side_effects=True),
         name="mixture",
     )(
-        heads, residual, norm_gain.reshape(1, width), routed_experts.T, route_weights.T,
+        heads, arrived, residual, norm_gain.reshape(1, width), routed_experts, route_weights.T,
         out_weight, shared_gate, shared_up, shared_down, expert_gate, expert_up, expert_down,
     )
 
@@ -537,9 +667,11 @@
     routed_experts,
     route_weights,
 ):
-    heads = attention(queries, key_heads, value_heads, head_gain)
+    experts = routed_experts.T
+    heads, arrived = attention(queries, key_heads, value_heads, head_gain, residual, experts)
     return mixture(
         heads,
+        arrived,
         residual,
         out_weight,
         norm_gain,
@@ -549,7 +681,7 @@
         expert_gate,
         expert_up,
         expert_down,
-        routed_experts,
+        experts,
         route_weights,
     )
 

time: 168 us -> 153 us (0.911)
  Pallas kernels: 162 us -> 150 us
  local copies, waits for them, and re-layouts: 6.41 us -> 1.88 us
    pallas_call x1, Pallas kernels: 97.6 us -> 78.5 us  [mixture(): pl.pallas_call(mixture_kernel, out_shape=jax.ShapeDtypeStruct((tokens, wi...]
    pallas_call x1, Pallas kernels: 63.9 us -> 71.9 us  [attention(): pl.pallas_call(attention_kernel, out_shape=(jax.ShapeDtypeStruct((128, 8...]
    unnamed x8 -> x1, local copies, waits for them, and re-layouts: 6.41 us -> 1.88 us
where the time goes in v5:
time: 153 us; the launch traced here: 152 us
  Pallas kernels  150 us (98%)
  local copies, waits for them, and re-layouts  1.88 us (1%)
    pallas_call x1, Pallas kernels, mixture(): pl.pallas_call(mixture_kernel, out_shape=jax.ShapeDtypeStruct((tokens, wi...  78.5 us
    pallas_call x1, Pallas kernels, attention(): pl.pallas_call(attention_kernel, out_shape=(jax.ShapeDtypeStruct((128, 8...  71.9 us

profile of v5, /device:TPU:1, one launch (start us, length us, event | category | flops | bytes accessed | tf_op | source)
XLA Modules:
  0.0 152.3 jit_solution(13453759914443132114)
XLA Ops:
  0.0 71.9 %attention.1 = (bf16[128,512]{1,0:T(8,128)(2,1)}, bf16[128,48,128]{2,1,0:T(8,128)(2,1)}) custom-call(bf16[64,1024]{1,0:T(8,128)(2,1)} %bitcast.7, bf16[64,1024]{1,0:T(8,128)(2,1)} %bitcast.8, bf16[64,1024]{1,0:T(8,128)(2,1)} %bitcast.9, f32[1,64]{1,0:T(1,128)} %bitcast.14, bf16[128,2048]{1,0:T(8,128)(2,1)} %residual_ref.3, s32[4,128]{1,0:T(4,128)} %bitcast.11), custom_call_target="tpu_custom_call" | custom-call | tf_op jit(solution)/shard_map/attention/pallas_call | solution.py:361
  71.9 78.5 %mixture.1 = bf16[128,2048]{1,0:T(8,128)(2,1)} custom-call(bf16[128,512]{1,0:T(8,128)(2,1)} %get-tuple-element.7.head_ref, bf16[128,48,128]{2,1,0:T(8,128)(2,1)} %get-tuple-element.8.arrived, bf16[128,2048]{1,0:T(8,128)(2,1)} %residual_ref.3, f32[1,2048]{1,0:T(1,128)} %bitcast.10, s32[4,128]{1,0:T(4,128)} %bitcast.12, f32[4,128]{1,0:T(4,128)} %bitcast.13, ...), custom_call_target="tpu_custom_call" | custom-call | tf_op jit(solution)/shard_map/mixture/pallas_call | solution.py:605
  150.4 1.9 %copy.17 = bf16[128,2048]{1,0:T(8,128)(2,1)} copy(bf16[128,2048]{1,0:T(8,128)(2,1)} %mixture.1) | data formatting | bytes 1048576

commit v6 on v5

--- a/solution.py
+++ b/solution.py
@@ -427,7 +427,7 @@
     for one in loads:
         one.start()
 
-    route(expert_ref, route_ref, place_ref, mix_ref)
+    route(expert_ref, None, place_ref, None)
     head_stage[...] = jnp.zeros_like(head_stage)
     for slot in range(slots):
         rows = jnp.dot(place_ref[0, slot], head_ref[...], preferred_element_type=f32)
@@ -442,6 +442,7 @@
 
     lax.fori_loop(0, devices // 8, pack, 0)
     spread(head_out, head_in, head_send, head_recv, head_local, me)
+    route(expert_ref, route_ref, place_ref, mix_ref)
 
     loads[0].wait()
     squares = jnp.zeros((tokens, 1), f32)

time: 153 us -> 153 us (level)
  no operation moved by 1% of the time
where the time goes in v6:
time: 153 us; the launch traced here: 152 us
  Pallas kernels  150 us (98%)
  local copies, waits for them, and re-layouts  1.88 us (1%)
    pallas_call x1, Pallas kernels, mixture(): pl.pallas_call(mixture_kernel, out_shape=jax.ShapeDtypeStruct((tokens, wi...  78.5 us
    pallas_call x1, Pallas kernels, attention(): pl.pallas_call(attention_kernel, out_shape=(jax.ShapeDtypeStruct((128, 8...  71.9 us

profile of v6, /device:TPU:1, one launch (start us, length us, event | category | flops | bytes accessed | tf_op | source)
XLA Modules:
  0.0 152.3 jit_solution(710527673269688441)
XLA Ops:
  0.0 71.9 %attention.1 = (bf16[128,512]{1,0:T(8,128)(2,1)}, bf16[128,48,128]{2,1,0:T(8,128)(2,1)}) custom-call(bf16[64,1024]{1,0:T(8,128)(2,1)} %bitcast.7, bf16[64,1024]{1,0:T(8,128)(2,1)} %bitcast.8, bf16[64,1024]{1,0:T(8,128)(2,1)} %bitcast.9, f32[1,64]{1,0:T(1,128)} %bitcast.14, bf16[128,2048]{1,0:T(8,128)(2,1)} %residual_ref.3, s32[4,128]{1,0:T(4,128)} %bitcast.11), custom_call_target="tpu_custom_call" | custom-call | tf_op jit(solution)/shard_map/attention/pallas_call | solution.py:361
  71.9 78.5 %mixture.1 = bf16[128,2048]{1,0:T(8,128)(2,1)} custom-call(bf16[128,512]{1,0:T(8,128)(2,1)} %get-tuple-element.7.head_ref, bf16[128,48,128]{2,1,0:T(8,128)(2,1)} %get-tuple-element.8.arrived, bf16[128,2048]{1,0:T(8,128)(2,1)} %residual_ref.3, f32[1,2048]{1,0:T(1,128)} %bitcast.10, s32[4,128]{1,0:T(4,128)} %bitcast.12, f32[4,128]{1,0:T(4,128)} %bitcast.13, ...), custom_call_target="tpu_custom_call" | custom-call | tf_op jit(solution)/shard_map/mixture/pallas_call | solution.py:606
  150.4 1.9 %copy.17 = bf16[128,2048]{1,0:T(8,128)(2,1)} copy(bf16[128,2048]{1,0:T(8,128)(2,1)} %mixture.1) | data formatting | bytes 1048576
